TPU v7x, 32 devices: a whole 2x2x4 slice. The times are simulated.
32 devices in a mesh: sp: 8 (over z, y), tp: 4 (over x, core).
Axes of the slice: x: 2, y: 2, z: 4, core: 2. Of those that a mesh axis runs over, the one named last changes fastest.
Arguments:
- tokens: bfloat16 [8192, 2048], P('sp', 'tp'), may hold values from -6 to 6
- input_norm_gain: float32 [2048], replicated, may hold values from 0.1 to 1.9
- pooling_input_matrix: bfloat16 [2048, 512], P(None, 'tp'), may hold values from -0.125 to 0.125
- query_projection_matrix: bfloat16 [2048, 1024], P(None, 'tp'), may hold values from -0.125 to 0.125
- key_projection_matrix: bfloat16 [2048, 1024], P(None, 'tp'), may hold values from -0.125 to 0.125
- value_projection_matrix: bfloat16 [2048, 1024], P(None, 'tp'), may hold values from -0.125 to 0.125
- output_gate_matrix: bfloat16 [2048, 1024], P(None, 'tp'), may hold values from -0.125 to 0.125
- input_gate_matrix: bfloat16 [2048, 2, 8], replicated
- forget_gate_matrix: bfloat16 [2048, 2, 8], replicated, may hold values from -0.125 to 0.125
- forget_gate_bias: float32 [2, 8], replicated
- log_forget_scale: float32 [2, 8192], P(None, 'sp'), may hold values from 0.35 to 2.8
- extra_log_forget: float32 [2, 8192], P(None, 'sp'), may hold values from -0.7 to 0, as said below
- starting_memory: float32 [2, 8, 128, 128], P(None, 'tp'), may hold values from -3 to 3
- starting_normalizer: float32 [2, 8, 128], P(None, 'tp'), may hold values from -3 to 3
- starting_log_scale: float32 [2, 8], P(None, 'tp'), may hold values from 2 to 5
- pooling_group_map: bfloat16 [4, 128, 128], replicated, may hold values from -0.5 to 0.5
- pooling_channel_scale: float32 [512], replicated, may hold values from 0.1 to 1.9
- memory_head_gain: float32 [1024], replicated, may hold values from 0.1 to 1.9
- pooling_output_matrix: bfloat16 [512, 2048], replicated, may hold values from -0.25 to 0.25
- memory_output_matrix: bfloat16 [1024, 2048], replicated, may hold values from -0.1875 to 0.1875
Outputs:
- mixed_out: bfloat16 [8192, 2048], P(('sp', 'tp'))
Inputs may be any that keep to these rules, and one draw needn't show every extreme that they name: `extra_log_forget`: at most three nonzero entries in each direction.
All inputs are finite; a program needn't handle non-finite values.
Results may differ from a plain program's by a relative error of at most 0.0091.
Values may be sent and summed in bfloat16 or wider, within the bound.
A program may use at most 128 MiB of HBM per device.

v0:
```python
import functools

import jax
import jax.numpy as jnp
from jax import lax
from jax.experimental import pallas as pl
from jax.experimental.pallas import tpu as pltpu
from jax.sharding import PartitionSpec as P

DH = 128
NEG_BIG = -1e30
LN_EPS = 1e-05
HEAD_EPS = 1e-06
RIM = 16
AUG = 144
VMEM = pltpu.VMEM
MESH = pl.DeviceIdType.MESH
F32 = jnp.float32
BF16 = jnp.bfloat16


def whole_vmem(count):
    return [pl.BlockSpec(memory_space=pltpu.VMEM)] * count


def scan_lanes(values, combine, neutral, forward_rows):
    lanes = values.shape[1]
    lane = lax.broadcasted_iota(jnp.int32, values.shape, 1)
    forward = lax.broadcasted_iota(jnp.int32, values.shape, 0) < forward_rows
    shift = 1
    while shift < lanes:
        low = jnp.where(lane >= shift, pltpu.roll(values, shift, 1), neutral)
        high = jnp.where(lane < lanes - shift, pltpu.roll(values, lanes - shift, 1), neutral)
        values = combine(values, jnp.where(forward, low, high))
        shift *= 2
    return values


def layer_kernel(
    tp_size, sp_size, heads,
    tokens_ref, gain_ref, gin_ref, gfg_ref, scale_ref, extra_ref, bias_ref,
    start_mem, start_norm, start_log, map_ref, pscale_ref, hgain_ref,
    wp_hbm, wq_hbm, wk_hbm, wv_hbm, wo_hbm, wpo_hbm, wmo_hbm,
    out_ref,
    held, normed, gate_w, wp, wq, wk, wv, wo, wpo, wmo,
    ext, q_ref, k_ref, v_ref, o_ref, gates_ref,
    adds, a_ref, acol_ref, ends_ref, locals_ref, inc_t, inc_s, exc_t, exc_s,
    send_t, send_s, recv_t, recv_s, rim_out, rims, enter_t, enter_s,
    pool_out, mem_out, lhs_pool, lhs_mem, acc,
    load_sem, far_send, far_recv, near_send, near_recv, pass_send, pass_recv,
    ts, tr, ss, sr, rs, rr, ps, pr, ms, mr,
):
    me = lax.axis_index("sp")
    group = lax.axis_index("tp")
    far = lax.rem(group + tp_size // 2, tp_size)
    near = group + 1 - 2 * lax.rem(group, 2)
    diagonal = lax.rem(near + tp_size // 2, tp_size)
    others = (far, diagonal, near)
    rows_total, width = tokens_ref.shape
    model_width = width * tp_size
    blocks = tp_size
    size = rows_total // blocks
    pairs = 2 * heads
    all_heads = gin_ref.shape[1]
    group_dim = map_ref.shape[1]
    mem_width = heads * DH
    strides = []
    stride = 1
    while stride < sp_size:
        strides.append(stride)
        stride *= 2

    barrier = pltpu.get_barrier_semaphore()
    peers = jnp.int32(len(others))
    for other in others:
        pl.semaphore_signal(barrier, inc=1, device_id={"tp": other}, device_id_type=MESH)
    for stride in strides:
        for okay, other in ((me + stride < sp_size, me + stride), (me >= stride, me - stride)):
            peers = peers + okay.astype(jnp.int32)

            @pl.when(okay)
            def _():
                pl.semaphore_signal(barrier, inc=1, device_id={"sp": other}, device_id_type=MESH)

    def load_group(pairs_of, first):
        copies = [
            pltpu.make_async_copy(source, target, load_sem.at[first + i])
            for i, (source, target) in enumerate(pairs_of)
        ]
        for copy in copies:
            copy.start()
        return copies

    loads = load_group(((wp_hbm, wp), (wq_hbm, wq), (wk_hbm, wk), (wv_hbm, wv), (wo_hbm, wo)), 0)
    gate_w[...] = jnp.concatenate(
        [ref[r].astype(F32) for ref in (gin_ref, gfg_ref) for r in range(2)], axis=0
    ).astype(BF16)
    pl.semaphore_wait(barrier, peers)

    def to_tp(source, target, send, recv, other):
        return pltpu.make_async_remote_copy(
            src_ref=source, dst_ref=target, send_sem=send, recv_sem=recv,
            device_id={"tp": other}, device_id_type=MESH,
        )

    def to_sp(source, target, send, recv, other):
        return pltpu.make_async_remote_copy(
            src_ref=source, dst_ref=target, send_sem=send, recv_sem=recv,
            device_id={"sp": other}, device_id_type=MESH,
        )

    spans = [pl.ds(c * size, size) for c in range(blocks)]
    to_far = [
        to_tp(tokens_ref.at[s], held.at[1, s], far_send.at[c], far_recv.at[c], far)
        for c, s in enumerate(spans)
    ]
    to_near = [
        to_tp(tokens_ref.at[s], held.at[0, s], near_send.at[c], near_recv.at[c], near)
        for c, s in enumerate(spans)
    ]
    onward = [
        to_tp(held.at[1, s], held.at[2, s], pass_send.at[c], pass_recv.at[c], near)
        for c, s in enumerate(spans)
    ]
    for c in range(blocks):
        to_far[c].start()
    for c in range(blocks):
        to_near[c].start()
    late_loads = load_group(((wpo_hbm, wpo), (wmo_hbm, wmo)), 5)

    bias_lane = lax.broadcasted_iota(jnp.int32, bias_ref.shape, 1)
    picked = [
        jnp.sum(jnp.where(bias_lane == group * heads + h, bias_ref[...], 0.0), axis=1, keepdims=True)
        for h in range(heads)
    ]
    bias = jnp.concatenate([picked[h][r : r + 1] for r in range(2) for h in range(heads)], axis=0)

    def own_gates(kind):
        parts = []
        for r in range(2):
            base = (2 * kind + r) * all_heads
            mine = gates_ref[base : base + heads, :]
            for other in range(1, tp_size):
                at = base + other * heads
                mine = jnp.where(group == other, gates_ref[at : at + heads, :], mine)
            parts.append(mine)
        return jnp.concatenate(parts, axis=0)

    def both_rows(ref, span):
        return jnp.concatenate(
            [jnp.broadcast_to(ref[r : r + 1, span], (heads, size)) for r in range(2)], axis=0
        )

    def project(c):
        rows = spans[c]
        views = [tokens_ref[rows, :]] + [held[slot, rows, :] for slot in range(3)]
        total = jnp.zeros((size, 1), F32)
        square = jnp.zeros((size, 1), F32)
        for view in views:
            part = view.astype(F32)
            total = total + jnp.sum(part, axis=1, keepdims=True)
            square = square + jnp.sum(part * part, axis=1, keepdims=True)
        mean = total / model_width
        inverse = lax.rsqrt(square / model_width - mean * mean + LN_EPS)
        for view, owner in zip(views, (group, near, far, diagonal)):
            columns = pl.ds(pl.multiple_of(owner * width, width), width)
            normed[:, columns] = (
                (view.astype(F32) - mean) * inverse * gain_ref[:, columns]
            ).astype(BF16)
        if c == 0:
            for load in loads:
                load.wait()
        x = normed[...]
        for weight, target in ((wk, k_ref), (wv, v_ref), (wq, q_ref), (wo, o_ref)):
            target[rows, :] = jnp.dot(x, weight[...], preferred_element_type=F32).astype(BF16)
        gates_ref[...] = lax.dot_general(
            gate_w[...], x, (((1,), (1,)), ((), ())), preferred_element_type=F32
        )
        pool = jnp.dot(x, wp[...], preferred_element_type=F32).astype(BF16)
        ext[pl.ds(RIM + c * size, size), :] = pool.astype(F32)
        if c == 0:
            rim_out[1] = pool[:RIM]
        if c == blocks - 1:
            rim_out[0] = pool[size - RIM :]

    def local_block(b):
        span = slice(b * size, (b + 1) * size)
        pre = own_gates(1) + bias
        log_sig = jnp.minimum(pre, 0.0) - jnp.log1p(jnp.exp(-jnp.abs(pre)))
        log_fg = log_sig * both_rows(scale_ref, span) + both_rows(extra_ref, span)
        falls = scan_lanes(log_fg, jnp.add, 0.0, heads)
        lifted = own_gates(0) - falls
        peaks = scan_lanes(lifted, jnp.maximum, NEG_BIG, heads)
        sources = lifted + jnp.log(F32(DH ** -0.5))
        columns = jnp.transpose(
            jnp.concatenate([peaks, jnp.zeros((128 - pairs, size), F32)], axis=0)
        )
        acol_ref[span, :] = columns
        t_at = lax.broadcasted_iota(jnp.int32, (size, size), 0)
        s_at = lax.broadcasted_iota(jnp.int32, (size, size), 1)
        for h in range(heads):
            cols = slice(h * DH, (h + 1) * DH)
            keys = k_ref[span, cols]
            vt = jnp.concatenate(
                [jnp.transpose(v_ref[span, cols].astype(F32)), jnp.ones((AUG - DH, size), F32)], axis=0
            )
            scores = lax.dot_general(
                q_ref[span, cols], keys, (((1,), (1,)), ((), ())), preferred_element_type=F32
            )
            values = jnp.concatenate([v_ref[span, cols], jnp.ones((size, DH), BF16)], axis=1)
            for r in range(2):
                p = r * heads + h
                end = size - 1 if r == 0 else 0
                top = peaks[p : p + 1, end : end + 1]
                ends_ref[b, p : p + 1, :] = jnp.broadcast_to(top, (1, 128))
                ends_ref[b, pairs + p : pairs + p + 1, :] = jnp.broadcast_to(
                    falls[p : p + 1, end : end + 1], (1, 128)
                )
                adds[p, b] = jnp.dot(
                    (vt * jnp.exp(sources[p : p + 1] - top)).astype(BF16), keys,
                    preferred_element_type=F32,
                )
                inside = (s_at <= t_at) if r == 0 else (s_at >= t_at)
                weight = jnp.exp(
                    jnp.where(inside, sources[p : p + 1] - columns[:, p : p + 1], NEG_BIG)
                )
                locals_ref[p, span, :] = jnp.dot(
                    (scores * weight).astype(BF16), values, preferred_element_type=F32
                )

    for c in range(blocks):
        to_far[c].wait_recv()
        onward[c].start()
        to_near[c].wait_recv()
        onward[c].wait_recv()
        project(c)
        local_block(c)

    def advance(p, b, state, level):
        peak = ends_ref[b, p : p + 1, :]
        fall = ends_ref[b, pairs + p : pairs + p + 1, :]
        top = jnp.maximum(level, peak)
        state = jnp.exp(level - top) * state + jnp.exp(peak - top) * adds[p, b]
        return (state, top + fall, fall)

    order = (tuple(range(blocks)), tuple(reversed(range(blocks))))
    for r in range(2):
        for h in range(heads):
            p = r * heads + h
            state = jnp.zeros((AUG, DH), F32)
            level = jnp.full((1, 128), NEG_BIG, F32)
            total_fall = jnp.zeros((1, 128), F32)
            for b in order[r]:
                state, level, fall = advance(p, b, state, level)
                total_fall = total_fall + fall
            inc_t[p] = state
            inc_s[r, h : h + 1, :] = level
            inc_s[r, heads + h : heads + h + 1, :] = total_fall
            exc_t[p] = jnp.zeros((AUG, DH), F32)
            exc_s[r, h : h + 1, :] = jnp.full((1, 128), NEG_BIG, F32)
            exc_s[r, heads + h : heads + h + 1, :] = jnp.zeros((1, 128), F32)

    def copies(level, r, other):
        return (
            to_sp(send_t.at[level, r], recv_t.at[level, r], ts.at[level, r], tr.at[level, r], other),
            to_sp(send_s.at[level, r], recv_s.at[level, r], ss.at[level, r], sr.at[level, r], other),
        )

    def route(level, r):
        stride = strides[level]
        if r == 0:
            return (me + stride < sp_size, me + stride, me >= stride)
        return (me >= stride, me - stride, me + stride < sp_size)

    def send(level):
        for r in range(2):
            okay, other, _unused = route(level, r)
            send_s[level, r] = inc_s[r]
            for h in range(heads):
                send_t[level, r, h] = inc_t[r * heads + h].astype(BF16)

            @pl.when(okay)
            def _():
                for copy in copies(level, r, other):
                    copy.start()

    def fold(level, r, t_ref, s_ref):
        for h in range(heads):
            p = r * heads + h
            early_max = recv_s[level, r, h : h + 1, :]
            early_fall = recv_s[level, r, heads + h : heads + h + 1, :]
            late_max = s_ref[r, h : h + 1, :]
            late_fall = s_ref[r, heads + h : heads + h + 1, :]
            top = jnp.maximum(early_max + late_fall, late_max)
            t_ref[p] = (
                jnp.exp(early_max + late_fall - top) * recv_t[level, r, h].astype(F32)
                + jnp.exp(late_max - top) * t_ref[p]
            )
            s_ref[r, h : h + 1, :] = top
            s_ref[r, heads + h : heads + h + 1, :] = early_fall + late_fall

    def receive(level, t_ref, s_ref, first):
        for r in range(2):
            okay, other, has = route(level, r)

            @pl.when(has)
            def _():
                if first:
                    for copy in copies(level, r, other):
                        copy.wait_recv()
                fold(level, r, t_ref, s_ref)

    def rim(side):
        other = me + 1 if side == 0 else me - 1
        return to_sp(rim_out.at[side], rims.at[side], rs.at[side], rr.at[side], other)

    rim_sends = (me + 1 < sp_size, me >= 1)
    rim_recvs = (me >= 1, me + 1 < sp_size)

    def pooling():
        for side in range(2):
            at = 0 if side == 0 else RIM + rows_total

            @pl.when(rim_recvs[side])
            def _():
                rim(side).wait_recv()
                ext[at : at + RIM, :] = rims[side].astype(F32)

            @pl.when(jnp.logical_not(rim_recvs[side]))
            def _():
                ext[at : at + RIM, :] = jnp.zeros((RIM, group_dim), F32)
        own = ext[RIM : RIM + rows_total, :]
        half = jnp.left_shift(jnp.int32(1), group)
        pooled = jnp.zeros_like(own)
        reach = RIM // 2
        for offset in range(-reach, reach):
            use = jnp.logical_and(offset >= -half, offset < half).astype(F32)
            pooled = pooled + use * ext[RIM + offset : RIM + offset + rows_total, :]
        position = me * rows_total + lax.broadcasted_iota(jnp.int32, own.shape, 0)
        count = jnp.minimum(position + half, rows_total * sp_size) - jnp.maximum(position - half, 0)
        contrast = (pooled / count.astype(F32) - own).astype(BF16)
        mapped = jnp.dot(contrast, map_ref[group], preferred_element_type=F32)
        scale = pscale_ref[:, pl.ds(pl.multiple_of(group * group_dim, group_dim), group_dim)]
        pool_out[...] = (mapped * scale).astype(BF16)

    pool_cols = pl.ds(pl.multiple_of(group * group_dim, group_dim), group_dim)
    mem_cols = pl.ds(pl.multiple_of(group * mem_width, mem_width), mem_width)

    def rows_of(owner):
        return pl.ds(pl.multiple_of(owner * size, size), size)

    pool_copies = [
        to_tp(pool_out.at[rows_of(other)], lhs_pool.at[:, pool_cols], ps.at[j], pr.at[j], other)
        for j, other in enumerate(others)
    ]
    mem_copies = [
        to_tp(mem_out.at[rows_of(other)], lhs_mem.at[:, mem_cols], ms.at[j], mr.at[j], other)
        for j, other in enumerate(others)
    ]

    def pool_product():
        lhs_pool[:, pool_cols] = pool_out[rows_of(group), :]
        for copy in pool_copies:
            copy.wait_recv()
        for load in late_loads:
            load.wait()
        acc[...] = jnp.dot(lhs_pool[...], wpo[...], preferred_element_type=F32)

    def start_pool():
        pooling()
        for copy in pool_copies:
            copy.start()

    send(0)
    for side in range(2):
        @pl.when(rim_sends[side])
        def _():
            rim(side).start()
    between = [start_pool] + [lambda: None] * len(strides)
    if len(strides) > 1:
        between[len(strides) - 1] = pool_product
    for level in range(len(strides)):
        if level > 0:
            send(level)
            receive(level - 1, exc_t, exc_s, False)
        between[level]()
        if level + 1 < len(strides):
            receive(level, inc_t, inc_s, True)
        else:
            receive(level, exc_t, exc_s, True)
    if len(strides) < 2:
        pool_product()

    for r in range(2):
        for h in range(heads):
            p = r * heads + h
            begin = start_log[r : r + 1, h : h + 1]
            late_max = exc_s[r, h : h + 1, :]
            late_fall = exc_s[r, heads + h : heads + h + 1, :]
            level = jnp.maximum(begin + late_fall, late_max)
            early = jnp.exp(begin + late_fall - level)
            late = jnp.exp(late_max - level)
            first = jnp.concatenate(
                [start_mem[r, h], jnp.broadcast_to(start_norm[r, h : h + 1, :], (AUG - DH, DH))], axis=0
            )
            state = early * first + late * exc_t[p]
            for n, b in enumerate(order[r]):
                enter_t[p, b] = jnp.concatenate(
                    [state[:DH], jnp.broadcast_to(state[DH : DH + 1], (DH, DH))], axis=0
                ).astype(BF16)
                enter_s[b, p : p + 1, :] = level
                if n + 1 < blocks:
                    state, level, _unused = advance(p, b, state, level)

    def finish(b, target, target_rows, target_cols):
        rows = rows_of(b)
        columns = acol_ref[rows, :]
        for h in range(heads):
            cols = slice(h * DH, (h + 1) * DH)
            queries = q_ref[rows, cols]
            hidden = jnp.zeros((size, DH), F32)
            for r in range(2):
                p = r * heads + h
                top = enter_s[b, p : p + 1, 0:1]
                peak = columns[:, p : p + 1]
                joint = jnp.maximum(peak, top)
                full = jnp.exp(peak - joint) * locals_ref[p, rows, :] + jnp.exp(
                    top - joint
                ) * lax.dot_general(
                    queries, enter_t[p, b], (((1,), (1,)), ((), ())), preferred_element_type=F32
                )
                hidden = hidden + full[:, :DH] / jnp.maximum(jnp.abs(full[:, DH:]), 1.0)
            centered = hidden - jnp.mean(hidden, axis=1, keepdims=True)
            variance = jnp.mean(centered * centered, axis=1, keepdims=True)
            gate = 1.0 / (1.0 + jnp.exp(-o_ref[rows, cols].astype(F32)))
            gain = hgain_ref[:, pl.ds(pl.multiple_of(group * mem_width + h * DH, DH), DH)]
            target[target_rows, target_cols(h)] = (
                centered * lax.rsqrt(variance + HEAD_EPS) * gain * gate
            ).astype(BF16)

    for other, copy in zip(others, mem_copies):
        finish(other, mem_out, rows_of(other), lambda h: slice(h * DH, (h + 1) * DH))
        copy.start()
    finish(
        group, lhs_mem, slice(None),
        lambda h: pl.ds(pl.multiple_of(group * mem_width + h * DH, DH), DH),
    )
    for copy in mem_copies:
        copy.wait_recv()
    tile = 512
    for n in range(out_ref.shape[1] // tile):
        cols = slice(n * tile, (n + 1) * tile)
        out_ref[:, cols] = (
            acc[:, cols] + jnp.dot(lhs_mem[...], wmo[:, cols], preferred_element_type=F32)
        ).astype(BF16)

    for c in range(blocks):
        to_far[c].wait_send()
        to_near[c].wait_send()
        onward[c].wait_send()
    for copy in pool_copies + mem_copies:
        copy.wait_send()
    for level in range(len(strides)):
        for r in range(2):
            okay, other, _unused = route(level, r)

            @pl.when(okay)
            def _():
                for copy in copies(level, r, other):
                    copy.wait_send()
    for side in range(2):
        @pl.when(rim_sends[side])
        def _():
            rim(side).wait_send()


def per_device(
    tokens,
    input_norm_gain,
    pooling_input_matrix,
    query_projection_matrix,
    key_projection_matrix,
    value_projection_matrix,
    output_gate_matrix,
    input_gate_matrix,
    forget_gate_matrix,
    forget_gate_bias,
    log_forget_scale,
    extra_log_forget,
    starting_memory,
    starting_normalizer,
    starting_log_scale,
    pooling_group_map,
    pooling_channel_scale,
    memory_head_gain,
    pooling_output_matrix,
    memory_output_matrix,
):
    rows, own_width = tokens.shape
    tp_size = lax.axis_size("tp")
    sp_size = lax.axis_size("sp")
    model_width = own_width * tp_size
    group_dim = pooling_input_matrix.shape[1]
    heads = query_projection_matrix.shape[1] // DH
    mem_width = heads * DH
    pairs = 2 * heads
    levels = max(1, (sp_size - 1).bit_length())
    blocks = tp_size
    size = rows // blocks
    all_heads = input_gate_matrix.shape[2]
    pool_total = pooling_output_matrix.shape[0]
    mem_total = memory_output_matrix.shape[0]
    anywhere = pl.BlockSpec(memory_space=pl.ANY)
    dma = pltpu.SemaphoreType.DMA
    return pl.pallas_call(
        functools.partial(layer_kernel, tp_size, sp_size, heads),
        out_shape=jax.ShapeDtypeStruct((size, model_width), BF16),
        in_specs=whole_vmem(13) + [anywhere] * 7,
        out_specs=pl.BlockSpec(memory_space=pltpu.VMEM),
        scratch_shapes=[
            VMEM((3, rows, own_width), BF16),
            VMEM((size, model_width), BF16),
            VMEM((4 * all_heads, model_width), BF16),
            VMEM((model_width, group_dim), BF16),
        ]
        + [VMEM((model_width, mem_width), BF16)] * 4
        + [
            VMEM((pool_total, model_width), BF16),
            VMEM((mem_total, model_width), BF16),
            VMEM((rows + 2 * RIM, group_dim), F32),
        ]
        + [VMEM((rows, mem_width), BF16)] * 4
        + [
            VMEM((4 * all_heads, size), F32),
            VMEM((pairs, blocks, AUG, DH), F32),
            VMEM((pairs, size), F32),
            VMEM((rows, 128), F32),
            VMEM((blocks, 2 * pairs, 128), F32),
            VMEM((pairs, rows, 2 * DH), F32),
            VMEM((pairs, AUG, DH), F32),
            VMEM((2, 2 * heads, 128), F32),
            VMEM((pairs, AUG, DH), F32),
            VMEM((2, 2 * heads, 128), F32),
            VMEM((levels, 2, heads, AUG, DH), BF16),
            VMEM((levels, 2, 2 * heads, 128), F32),
            VMEM((levels, 2, heads, AUG, DH), BF16),
            VMEM((levels, 2, 2 * heads, 128), F32),
            VMEM((2, RIM, group_dim), BF16),
            VMEM((2, RIM, group_dim), BF16),
            VMEM((pairs, blocks, 2 * DH, DH), BF16),
            VMEM((blocks, pairs, 128), F32),
            VMEM((rows, group_dim), BF16),
            VMEM((rows, mem_width), BF16),
            VMEM((size, pool_total), BF16),
            VMEM((size, mem_total), BF16),
            VMEM((size, model_width), F32),
        ]
        + [dma((7,))]
        + [dma((blocks,))] * 6
        + [dma((levels, 2))] * 4
        + [dma((2,))] * 2
        + [dma((3,))] * 4,
        compiler_params=pltpu.CompilerParams(
            collective_id=0, has_side_effects=True, vmem_limit_bytes=67043328
        ),
    )(
        tokens,
        input_norm_gain.reshape(1, model_width),
        input_gate_matrix.transpose(1, 2, 0),
        forget_gate_matrix.transpose(1, 2, 0),
        log_forget_scale,
        extra_log_forget,
        forget_gate_bias,
        starting_memory,
        starting_normalizer,
        starting_log_scale,
        pooling_group_map,
        pooling_channel_scale.reshape(1, pool_total),
        memory_head_gain.reshape(1, mem_total),
        pooling_input_matrix,
        query_projection_matrix,
        key_projection_matrix,
        value_projection_matrix,
        output_gate_matrix,
        pooling_output_matrix,
        memory_output_matrix,
    )


def solution(mesh):
    placed = (
        P("sp", "tp"),
        P(),
        P(None, "tp"),
        P(None, "tp"),
        P(None, "tp"),
        P(None, "tp"),
        P(None, "tp"),
        P(),
        P(),
        P(),
        P(None, "sp"),
        P(None, "sp"),
        P(None, "tp", None, None),
        P(None, "tp", None),
        P(None, "tp"),
        P(),
        P(),
        P(),
        P(),
        P(),
    )
    return jax.shard_map(
        per_device, mesh=mesh, in_specs=placed, out_specs=P(("sp", "tp"), None), check_vma=False
    )
```

profile of v0, /device:TPU:1, one launch (start us, length us, event | category | flops | bytes accessed | tf_op | source)
XLA Modules:
  0.0 63.0 jit_solution(18026602193698904490)
XLA Ops:
  0.0 60.7 %shard_map.190 = bf16[256,2048]{1,0:T(8,128)(2,1)} custom-call(bf16[1024,512]{1,0:T(8,128)(2,1)} %tokens_ref.1, f32[1,2048]{1,0:T(1,128)} %bitcast.7, bf16[2,8,2048]{2,1,0:T(8,128)(2,1)} %bitcast.5, bf16[2,8,2048]{2,1,0:T(8,128)(2,1)} %bitcast.6, f32[2,1024]{1,0:T(2,128)} %scale_ref.1, f32[2,1024]{1,0:T(2,128)} %extra_ref.1, f32[2,8]{1,0:T(2,128)} %bias_ref.1, ...), custom_call_target="tpu_custom_call" | custom-call | tf_op jit(solution)/shard_map/pallas_call | solution.py:515
  60.7 2.3 %copy.22 = bf16[256,2048]{1,0:T(8,128)(2,1)} copy(bf16[256,2048]{1,0:T(8,128)(2,1)} %shard_map.190) | data formatting | bytes 2097152
where the time goes:
time: 63.2 us; the launch traced here: 63 us
  Pallas kernels  60.7 us (96%)
  local copies, waits for them, and re-layouts  2.3 us (4%)
    pallas_call x1, Pallas kernels, per_device(): pl.pallas_call(functools.partial(layer_kernel, tp_size, sp_size, heads),...  60.7 us
    unnamed x1, local copies, waits for them, and re-layouts  2.3 us

commit v1 on v0

v1 whole, which is shorter than its diff:
```python
import contextlib
import functools
import types

import jax
import jax.numpy as jnp
from jax import lax
from jax.experimental import pallas as pl
from jax.experimental.pallas import tpu as pltpu
from jax.sharding import PartitionSpec as P

DH = 128
NEG_BIG = -1e30
LN_EPS = 1e-05
HEAD_EPS = 1e-06
RIM = 16
AUG = 144
VMEM = pltpu.VMEM
MESH = pl.DeviceIdType.MESH
F32 = jnp.float32
BF16 = jnp.bfloat16
PROFILE = False
KERNEL_VMEM = 48 * 1024 * 1024
SMALL = (
    "gin", "gfg", "gain", "scale", "extra", "bias", "start_mem", "start_norm", "start_log",
    "map", "pscale", "hgain",
)


def scope(name):
    return jax.named_scope(name) if PROFILE else contextlib.nullcontext()


def scan_lanes(values, combine, neutral, forward_rows):
    lanes = values.shape[1]
    lane = lax.broadcasted_iota(jnp.int32, values.shape, 1)
    forward = lax.broadcasted_iota(jnp.int32, values.shape, 0) < forward_rows
    shift = 1
    while shift < lanes:
        low = jnp.where(lane >= shift, pltpu.roll(values, shift, 1), neutral)
        high = jnp.where(lane < lanes - shift, pltpu.roll(values, lanes - shift, 1), neutral)
        values = combine(values, jnp.where(forward, low, high))
        shift *= 2
    return values


def split_three(values):
    high = values.astype(BF16)
    rest = values - high.astype(F32)
    middle = rest.astype(BF16)
    low = (rest - middle.astype(F32)).astype(BF16)
    return high.astype(F32), middle.astype(F32), low.astype(F32)


def wide(row, lanes):
    return jnp.concatenate([row] * (lanes // row.shape[1]), axis=1)


def layer_kernel(tp_size, sp_size, heads, names, *refs):
    k = types.SimpleNamespace(**dict(zip(names, refs, strict=True)))
    me = lax.axis_index("sp")
    group = lax.axis_index("tp")
    far = lax.rem(group + tp_size // 2, tp_size)
    near = group + 1 - 2 * lax.rem(group, 2)
    diagonal = lax.rem(near + tp_size // 2, tp_size)
    others = (far, diagonal, near)
    rows_total, width = k.tokens.shape
    small_refs = [(getattr(k, name + "_in"), getattr(k, name)) for name in SMALL]
    model_width = width * tp_size
    blocks = tp_size
    size = rows_total // blocks
    half = size // 2
    pairs = 2 * heads
    all_heads = k.gin.shape[1]
    group_dim = k.map.shape[1]
    mem_width = heads * DH
    last = blocks - 1
    odd = lax.rem(me, 2)
    partner = me + 1 - 2 * odd
    strides = [1]
    while strides[-1] * 2 < sp_size:
        strides.append(strides[-1] * 2)
    levels = len(strides)

    def route(level, r):
        stride = strides[level]
        if level == 0:
            return True, partner, True
        if r == 0:
            return me + stride < sp_size, me + stride, me >= stride
        return me >= stride, me - stride, me + stride < sp_size

    def when(condition):
        if condition is True:
            return lambda body: body()
        return pl.when(condition)

    rim_sends = (me + 1 < sp_size, me >= 1)
    rim_recvs = (me >= 1, me + 1 < sp_size)

    barrier = pltpu.get_barrier_semaphore()
    peers = jnp.int32(len(others))
    for other in others:
        pl.semaphore_signal(barrier, inc=1, device_id={"tp": other}, device_id_type=MESH)
    greets = []
    for stride in strides:
        greets += [(me + stride < sp_size, me + stride), (me >= stride, me - stride)]
    for okay, other in greets:
        peers = peers + okay.astype(jnp.int32)

        @pl.when(okay)
        def _():
            pl.semaphore_signal(barrier, inc=1, device_id={"sp": other}, device_id_type=MESH)

    spans = [(b * size, size) for b in range(last)]
    spans += [(last * size, half), (last * size + half, half)]
    token_loads = [
        pltpu.make_async_copy(k.tokens.at[pl.ds(a, n)], k.own.at[pl.ds(a, n)], k.token_sem.at[i])
        for i, (a, n) in enumerate(spans)
    ]
    for load in token_loads:
        load.start()

    def load_group(pairs_of, sems, first=0):
        copies = [
            pltpu.make_async_copy(source, target, sems.at[first + i])
            for i, (source, target) in enumerate(pairs_of)
        ]
        for copy in copies:
            copy.start()
        return copies

    smalls = load_group(small_refs, k.small_sem)
    loads = load_group(
        (
            (k.wp_hbm, k.wpg.at[:, pl.ds(0, group_dim)]),
            (k.wk_hbm, k.wk), (k.wv_hbm, k.wv), (k.wq_hbm, k.wq), (k.wo_hbm, k.wo),
        ),
        k.load_sem,
    )
    for load in smalls[:2]:
        load.wait()

    def own_rows(ref, r):
        mine = ref[r, 0:heads, :].astype(F32)
        for other in range(1, tp_size):
            mine = jnp.where(
                group == other, ref[r, other * heads : (other + 1) * heads, :].astype(F32), mine
            )
        return mine

    gate_rows = jnp.concatenate([own_rows(ref, r) for ref in (k.gin, k.gfg) for r in range(2)], axis=0)
    gate_rows = jnp.concatenate(
        [gate_rows, jnp.zeros((128 - 2 * pairs, model_width), F32)], axis=0
    )
    for n in range(model_width // 128):
        at = slice(n * 128, (n + 1) * 128)
        k.wpg[at, group_dim : group_dim + 128] = jnp.transpose(gate_rows[:, at]).astype(BF16)
    s_at = lax.broadcasted_iota(jnp.int32, (size, size), 0)
    t_at = lax.broadcasted_iota(jnp.int32, (size, size), 1)
    k.sums[:, 0:size] = (s_at <= t_at).astype(F32).astype(BF16)
    k.sums[:, size : 2 * size] = (s_at >= t_at).astype(F32).astype(BF16)

    with scope("barrier"):
        pl.semaphore_wait(barrier, peers)

    def to_tp(source, target, send, recv, other):
        return pltpu.make_async_remote_copy(
            src_ref=source, dst_ref=target, send_sem=send, recv_sem=recv,
            device_id={"tp": other}, device_id_type=MESH,
        )

    def to_sp(source, target, send, recv, other):
        return pltpu.make_async_remote_copy(
            src_ref=source, dst_ref=target, send_sem=send, recv_sem=recv,
            device_id={"sp": other}, device_id_type=MESH,
        )

    to_far, to_near, onward = [], [], []
    for i, (a, n) in enumerate(spans):
        s = pl.ds(a, n)
        to_far.append(to_tp(k.own.at[s], k.held.at[1, s], k.far_send.at[i], k.far_recv.at[i], far))
        to_near.append(to_tp(k.own.at[s], k.held.at[0, s], k.near_send.at[i], k.near_recv.at[i], near))
        onward.append(
            to_tp(k.held.at[1, s], k.held.at[2, s], k.pass_send.at[i], k.pass_recv.at[i], near)
        )
    for i in range(len(spans)):
        token_loads[i].wait()
        to_far[i].start()
    for i in range(len(spans)):
        to_near[i].start()
    mem_rows = [
        (k.wmo_hbm.at[pl.ds((g * heads + h) * DH, DH)], k.wmo.at[h, pl.ds(g * DH, DH)])
        for h in range(heads)
        for g in range(tp_size)
    ]
    late_loads = load_group([(k.wpo_hbm, k.wpo)] + mem_rows, k.late_sem)
    for load in smalls[2:]:
        load.wait()

    bias_lane = lax.broadcasted_iota(jnp.int32, k.bias.shape, 1)
    picked = [
        jnp.sum(jnp.where(bias_lane == group * heads + h, k.bias[...], 0.0), axis=1, keepdims=True)
        for h in range(heads)
    ]
    bias = jnp.concatenate([picked[h][r : r + 1] for r in range(2) for h in range(heads)], axis=0)

    def both_rows(ref, span):
        return jnp.concatenate(
            [jnp.broadcast_to(ref[r : r + 1, span], (heads, size)) for r in range(2)], axis=0
        )

    def normalize(a, n, at):
        rows = slice(a, a + n)
        views = [k.own[rows, :]] + [k.held[slot, rows, :] for slot in range(3)]
        total = jnp.zeros((n, 1), F32)
        square = jnp.zeros((n, 1), F32)
        for view in views:
            part = view.astype(F32)
            total = total + jnp.sum(part, axis=1, keepdims=True)
            square = square + jnp.sum(part * part, axis=1, keepdims=True)
        mean = total / model_width
        inverse = lax.rsqrt(square / model_width - mean * mean + LN_EPS)
        for view, owner in zip(views, (group, near, far, diagonal)):
            columns = pl.ds(pl.multiple_of(owner * width, width), width)
            k.normed[at : at + n, columns] = (
                (view.astype(F32) - mean) * inverse * k.gain[:, columns]
            ).astype(BF16)

    def project(a, n, at, targets):
        x = k.normed[at : at + n, :]
        for weight, target in targets:
            target[a : a + n, :] = jnp.dot(x, weight[...], preferred_element_type=F32).astype(BF16)

    def project_gates(a, n, at):
        x = k.normed[at : at + n, :]
        mixed = jnp.dot(x, k.wpg[...], preferred_element_type=F32)
        k.ext[RIM + a : RIM + a + n, :] = mixed[:, :group_dim].astype(BF16).astype(F32)
        k.gates[:, at : at + n] = jnp.transpose(mixed[:, group_dim:])[: 2 * pairs]

    zero_state = jnp.zeros((AUG, DH), F32)

    def initial(r, h):
        is_first = me == (0 if r == 0 else sp_size - 1)
        begin = jnp.broadcast_to(k.start_log[r : r + 1, h : h + 1], (1, 128))
        level = jnp.where(is_first, begin, NEG_BIG)
        rows = jnp.concatenate(
            [k.start_mem[r, h], jnp.broadcast_to(k.start_norm[r, h : h + 1, :], (AUG - DH, DH))], axis=0
        )
        return jnp.where(is_first, rows, 0.0), level

    def prepare():
        for h in range(heads):
            state, level = initial(0, h)
            k.cur_t[h] = state
            k.cur_s[h : h + 1, :] = level
            k.cur_t[heads + h] = zero_state
            k.cur_s[heads + h : heads + h + 1, :] = jnp.full((1, 128), NEG_BIG, F32)
        k.cur_s[pairs : 2 * pairs, :] = jnp.zeros((pairs, 128), F32)

    def summary(b):
        span = slice(b * size, (b + 1) * size)
        pre = k.gates[pairs : 2 * pairs, :] + bias
        log_sig = jnp.minimum(pre, 0.0) - jnp.log1p(jnp.exp(-jnp.abs(pre)))
        log_fg = log_sig * both_rows(k.scale, span) + both_rows(k.extra, span)
        parts = jnp.concatenate(split_three(log_fg), axis=0).astype(BF16)
        sums = jnp.dot(parts, k.sums[...], preferred_element_type=F32)
        sums = sums[:pairs] + sums[pairs : 2 * pairs] + sums[2 * pairs :]
        falls = jnp.concatenate([sums[:heads, :size], sums[heads:, size:]], axis=0)
        lifted = k.gates[:pairs, :] - falls
        top = jnp.max(lifted, axis=1, keepdims=True)
        sources = lifted + jnp.log(F32(DH ** -0.5))
        k.lifted[...] = lifted
        weights = jnp.exp(sources - top)
        peaks = jnp.broadcast_to(top, (pairs, 128))
        fall = jnp.concatenate(
            [falls[:heads, size - 1 : size], falls[heads:, 0:1]], axis=0
        )
        fall = jnp.broadcast_to(fall, (pairs, 128))
        for h in range(heads):
            cols = slice(h * DH, (h + 1) * DH)
            keys = k.k[span, cols]
            vt = jnp.concatenate(
                [jnp.transpose(k.v[span, cols].astype(F32)), jnp.ones((AUG - DH, size), F32)], axis=0
            )
            k.vt[h] = vt.astype(BF16)
            adds = [
                jnp.dot(
                    (vt * weights[p : p + 1]).astype(BF16), keys, preferred_element_type=F32
                )
                for p in (h, heads + h)
            ]
            p = h
            peak, down = peaks[p : p + 1], fall[p : p + 1]
            level = k.cur_s[p : p + 1, :]
            k.enter_t[0, h] = k.cur_t[p].astype(BF16)
            k.enter_s[0, h : h + 1, :] = level
            k.fcum[b, p : p + 1, :] = k.cur_s[pairs + p : pairs + p + 1, :]
            joint = jnp.maximum(level, peak)
            k.cur_t[p] = jnp.exp(level - joint) * k.cur_t[p] + jnp.exp(peak - joint) * adds[0]
            k.cur_s[p : p + 1, :] = joint + down
            k.cur_s[pairs + p : pairs + p + 1, :] += down
            p = heads + h
            peak, down = peaks[p : p + 1], fall[p : p + 1]
            k.ends[b, p : p + 1, :] = peak
            k.ends[b, pairs + p : pairs + p + 1, :] = down
            late = k.cur_s[p : p + 1, :]
            late_fall = k.cur_s[pairs + p : pairs + p + 1, :]
            if b < last:
                k.adds[h, b] = adds[1]
                early, level = adds[1], peak + down
            else:
                state, level = initial(1, h)
                k.back_t[h, b] = state.astype(BF16)
                k.back_s[b, h : h + 1, :] = level
                joint = jnp.maximum(level, peak)
                early = jnp.exp(level - joint) * state + jnp.exp(peak - joint) * adds[1]
                level = joint + down
                if b > 0:
                    k.back_f[h] = early
                    k.back_s[b - 1, h : h + 1, :] = level
            level = level + late_fall
            joint = jnp.maximum(level, late)
            k.cur_t[p] = jnp.exp(level - joint) * early + jnp.exp(late - joint) * k.cur_t[p]
            k.cur_s[p : p + 1, :] = joint
            k.cur_s[pairs + p : pairs + p + 1, :] = late_fall + down

    def local_block(b):
        span = slice(b * size, (b + 1) * size)
        lifted = k.lifted[...]
        peaks = scan_lanes(lifted, jnp.maximum, NEG_BIG, heads)
        levels_in = jnp.concatenate(
            [wide(k.enter_s[0, 0:heads, :], size), jnp.full((heads, size), NEG_BIG, F32)], axis=0
        )
        peaks = jnp.maximum(peaks, levels_in)
        k.peaks[b, 0:pairs, :] = peaks
        carry = jnp.exp(levels_in[:heads] - peaks[:heads])
        sources = lifted + jnp.log(F32(DH ** -0.5))
        columns = jnp.transpose(
            jnp.concatenate([sources, jnp.zeros((128 - pairs, size), F32)], axis=0)
        )
        for h in range(heads):
            cols = slice(h * DH, (h + 1) * DH)
            queries = k.q[span, cols]
            scores = lax.dot_general(
                k.k[span, cols], queries, (((1,), (1,)), ((), ())), preferred_element_type=F32
            )
            values = k.vt[h]
            before = lax.dot_general(
                k.enter_t[0, h], queries, (((1,), (1,)), ((), ())), preferred_element_type=F32
            )
            for r in range(2):
                p = r * heads + h
                inside = (s_at <= t_at) if r == 0 else (s_at >= t_at)
                weight = jnp.exp(
                    jnp.where(inside, columns[:, p : p + 1] - peaks[p : p + 1], NEG_BIG)
                )
                result = jnp.dot(
                    values, (scores * weight).astype(BF16), preferred_element_type=F32
                )
                if r == 0:
                    result = result + carry[h : h + 1] * before
                k.locals[p, b] = result

    def out_gates(b):
        span = slice(b * size, (b + 1) * size)
        for h in range(heads):
            opened = jnp.transpose(k.o[span, h * DH : (h + 1) * DH].astype(F32))
            gain = k.hgain[:, pl.ds(pl.multiple_of(group * mem_width + h * DH, DH), DH)]
            column = jnp.transpose(jnp.broadcast_to(gain, (128, DH)))
            k.gated[h, b] = wide(column, size) / (1.0 + jnp.exp(-opened))

    with scope("prepare"):
        prepare()
    for b in range(blocks):
        pieces = [i for i, (a, n) in enumerate(spans) if b * size <= a < (b + 1) * size]
        with scope(f"far{b}"):
            for i in pieces:
                to_far[i].wait_recv()
                onward[i].start()
        for i in pieces:
            a, n = spans[i]
            at = a - b * size
            with scope(f"wait{i}"):
                to_near[i].wait_recv()
                onward[i].wait_recv()
            if i == 0:
                for load in loads:
                    load.wait()
            with scope(f"project{i}"):
                normalize(a, n, at)
                project_gates(a, n, at)
                project(a, n, at, ((k.wk, k.k), (k.wv, k.v)))
        if b < last:
            with scope(f"local{b}"):
                project(b * size, size, 0, ((k.wq, k.q), (k.wo, k.o)))
                summary(b)
                local_block(b)
                out_gates(b)
        else:
            with scope(f"summary{b}"):
                summary(b)

    for r in range(2):
        for h in range(heads):
            p = r * heads + h
            k.inc_s[r, h : h + 1, :] = k.cur_s[p : p + 1, :]
            k.inc_s[r, heads + h : heads + h + 1, :] = k.cur_s[pairs + p : pairs + p + 1, :]

    def scalar_copy(level, r):
        return to_sp(
            k.send_s.at[level, r], k.recv_s.at[level, r], k.ss.at[level, r], k.sr.at[level, r],
            route(level, r)[1],
        )

    def state_copy(level, r, h):
        return to_sp(
            k.send_t.at[level, r, h], k.recv_t.at[level, r, h], k.ts.at[level, r, h],
            k.tr.at[level, r, h], route(level, r)[1],
        )

    def ready(slot, level, r):
        okay = route(level, r)[0]
        if slot >= 2:
            okay = jnp.logical_and(okay, route(slot - 1, r)[2])
        if level > slot:
            okay = jnp.logical_and(okay, jnp.logical_not(route(slot, r)[2]))
        return okay

    def send_scalars(slot):
        for r in range(2):
            for level in range(slot, levels if slot > 0 else 1):
                @when(ready(slot, level, r))
                def _():
                    k.send_s[level, r] = k.inc_s[r]
                    scalar_copy(level, r).start()

    def send_state(slot, r, h):
        for level in range(slot, levels if slot > 0 else 1):
            @when(ready(slot, level, r))
            def _():
                k.send_t[level, r, h] = k.cur_t[r * heads + h].astype(BF16)
                state_copy(level, r, h).start()

    def take_scalars(level):
        for r in range(2):
            @when(route(level, r)[2])
            def _():
                scalar_copy(level, r).wait_recv()
                theirs_max = k.recv_s[level, r, 0:heads, :]
                theirs_fall = k.recv_s[level, r, heads : 2 * heads, :]
                own_max = k.inc_s[r, 0:heads, :]
                own_fall = k.inc_s[r, heads : 2 * heads, :]
                if level == 0:
                    early = (odd == 1) if r == 0 else (odd == 0)
                    a = jnp.where(early, theirs_max + own_fall, theirs_max)
                    c = jnp.where(early, own_max, own_max + theirs_fall)
                    flag = jnp.where(early, 1.0, 0.0).astype(F32)
                    k.weigh[r, 2 * heads : 3 * heads, :] = jnp.full((heads, 128), flag, F32)
                    k.exc_s[r, 0:heads, :] = jnp.where(early, theirs_max, NEG_BIG)
                    k.exc_s[r, heads : 2 * heads, :] = jnp.where(early, theirs_fall, 0.0)
                else:
                    a = theirs_max + own_fall
                    c = own_max
                    late_max = k.exc_s[r, 0:heads, :]
                    late_fall = k.exc_s[r, heads : 2 * heads, :]
                    level_in = theirs_max + late_fall
                    top = jnp.maximum(level_in, late_max)
                    k.weigh[r, 2 * heads : 3 * heads, :] = jnp.exp(level_in - top)
                    k.weigh[r, 3 * heads : 4 * heads, :] = jnp.exp(late_max - top)
                    k.exc_s[r, 0:heads, :] = top
                    k.exc_s[r, heads : 2 * heads, :] = theirs_fall + late_fall
                top = jnp.maximum(a, c)
                k.weigh[r, 0:heads, :] = jnp.exp(a - top)
                k.weigh[r, heads : 2 * heads, :] = jnp.exp(c - top)
                k.inc_s[r, 0:heads, :] = top
                k.inc_s[r, heads : 2 * heads, :] = theirs_fall + own_fall

    def take_state(level, r, h):
        @when(route(level, r)[2])
        def _():
            state_copy(level, r, h).wait_recv()
            p = r * heads + h
            arrived = k.recv_t[level, r, h].astype(F32)
            if level + 1 < levels:
                k.cur_t[p] = (
                    k.weigh[r, h : h + 1, :] * arrived
                    + k.weigh[r, heads + h : heads + h + 1, :] * k.cur_t[p]
                )
            mine = k.weigh[r, 2 * heads + h : 2 * heads + h + 1, :] * arrived
            if level > 0:
                mine = mine + k.weigh[r, 3 * heads + h : 3 * heads + h + 1, :] * k.exc_t[p]
            k.exc_t[p] = mine

    def rim(side):
        other = me + 1 if side == 0 else me - 1
        return to_sp(k.rim_out.at[side], k.rims.at[side], k.rs.at[side], k.rr.at[side], other)

    def start_rims():
        k.rim_out[1] = k.ext[RIM : 2 * RIM, :].astype(BF16)
        k.rim_out[0] = k.ext[rows_total : RIM + rows_total, :].astype(BF16)
        for side in range(2):
            @pl.when(rim_sends[side])
            def _():
                rim(side).start()

    def pooling():
        for side in range(2):
            at = 0 if side == 0 else RIM + rows_total

            @pl.when(rim_recvs[side])
            def _():
                rim(side).wait_recv()
                k.ext[at : at + RIM, :] = k.rims[side].astype(F32)

            @pl.when(jnp.logical_not(rim_recvs[side]))
            def _():
                k.ext[at : at + RIM, :] = jnp.zeros((RIM, group_dim), F32)
        half_span = jnp.left_shift(jnp.int32(1), group)
        for n in range(blocks):
            first = n * size
            chunk = k.ext[first : first + size + 2 * RIM, :]
            own = chunk[RIM : RIM + size]
            low = 1
            running = chunk[: size + 2 * RIM - 1] + chunk[1:]
            reach = 1
            while 2 * reach < RIM:
                span = running.shape[0] - 2 * reach
                longer = running[:span] + running[2 * reach :]
                kept = running[reach : reach + span]
                running = jnp.where(half_span > reach, longer, kept)
                low += reach
                reach *= 2
            pooled = running[RIM - low : RIM - low + size]
            position = me * rows_total + first + lax.broadcasted_iota(jnp.int32, own.shape, 0)
            count = jnp.minimum(position + half_span, rows_total * sp_size) - jnp.maximum(
                position - half_span, 0
            )
            contrast = (pooled / count.astype(F32) - own).astype(BF16)
            mapped = jnp.dot(contrast, k.map[group], preferred_element_type=F32)
            scale = k.pscale[:, pl.ds(pl.multiple_of(group * group_dim, group_dim), group_dim)]
            k.pool_out[first : first + size, :] = (mapped * scale).astype(BF16)

    pool_cols = pl.ds(pl.multiple_of(group * group_dim, group_dim), group_dim)

    def rows_of(owner):
        return pl.ds(pl.multiple_of(owner * size, size), size)

    own_cols = pl.ds(pl.multiple_of(group * DH, DH), DH)

    pool_copies = [
        to_tp(k.pool_out.at[rows_of(other)], k.lhs_pool.at[:, pool_cols], k.ps.at[j], k.pr.at[j], other)
        for j, other in enumerate(others)
    ]
    mem_copies = [
        [
            to_tp(
                k.mem_out.at[h, rows_of(other)], k.lhs_mem.at[h, :, own_cols],
                k.ms.at[h, j], k.mr.at[h, j], other,
            )
            for j, other in enumerate(others)
        ]
        for h in range(heads)
    ]

    def start_pool():
        pooling()
        for copy in pool_copies:
            copy.start()

    def pool_product():
        k.lhs_pool[:, pool_cols] = k.pool_out[rows_of(group), :]
        for copy in pool_copies:
            copy.wait_recv()
        for load in late_loads:
            load.wait()
        k.acc[...] = jnp.dot(k.lhs_pool[...], k.wpo[...], preferred_element_type=F32)

    def last_local():
        project(last * size, size, 0, ((k.wq, k.q), (k.wo, k.o)))
        local_block(last)
        out_gates(last)

    def backward_enter():
        for h in range(heads):
            p = heads + h
            fall = k.ends[last, pairs + p : pairs + p + 1, :]
            k.fcum[last, p : p + 1, :] = jnp.zeros((1, 128), F32)
            if blocks > 1:
                state, level = k.back_f[h], k.back_s[last - 1, h : h + 1, :]
            for b in reversed(range(last)):
                k.back_t[h, b] = state.astype(BF16)
                k.fcum[b, p : p + 1, :] = fall
                if b > 0:
                    peak = k.ends[b, p : p + 1, :]
                    down = k.ends[b, pairs + p : pairs + p + 1, :]
                    joint = jnp.maximum(level, peak)
                    state = jnp.exp(level - joint) * state + jnp.exp(peak - joint) * k.adds[h, b]
                    level = joint + down
                    k.back_s[b - 1, h : h + 1, :] = level
                    fall = fall + down
        for b in range(blocks):
            span = slice(b * size, (b + 1) * size)
            for h in range(heads):
                p = heads + h
                level = wide(k.back_s[b, h : h + 1, :], size)
                peak = k.peaks[b, p : p + 1, :]
                joint = jnp.maximum(level, peak)
                before = lax.dot_general(
                    k.back_t[h, b], k.q[span, h * DH : (h + 1) * DH], (((1,), (1,)), ((), ())),
                    preferred_element_type=F32,
                )
                k.locals[p, b] = (
                    jnp.exp(peak - joint) * k.locals[p, b] + jnp.exp(level - joint) * before
                )
                k.peaks[b, p : p + 1, :] = joint

    def finish(b, h):
        states = jnp.concatenate([k.exc_t[h], k.exc_t[heads + h]], axis=0).astype(BF16)
        queries = k.q[rows_of(b), h * DH : (h + 1) * DH]
        entered = lax.dot_general(
            states, queries, (((1,), (1,)), ((), ())), preferred_element_type=F32
        )
        hidden = None
        for r in range(2):
            p = r * heads + h
            level = wide(k.exc_s[r, h : h + 1, :] + k.fcum[b, p : p + 1, :], size)
            peak = k.peaks[b, p : p + 1, :]
            joint = jnp.maximum(level, peak)
            a = jnp.exp(peak - joint)
            c = jnp.exp(level - joint)
            mine = k.locals[p, b]
            theirs = entered[r * AUG : (r + 1) * AUG]
            below = a * mine[DH : DH + 1] + c * theirs[DH : DH + 1]
            inverse = 1.0 / jnp.maximum(jnp.abs(below), 1.0)
            part = (a * inverse) * mine[:DH] + (c * inverse) * theirs[:DH]
            hidden = part if hidden is None else hidden + part
        centered = hidden - jnp.mean(hidden, axis=0, keepdims=True)
        variance = jnp.mean(centered * centered, axis=0, keepdims=True)
        scaled = centered * lax.rsqrt(variance + HEAD_EPS) * k.gated[h, b]
        return jnp.transpose(scaled).astype(BF16)

    with scope("send0"):
        send_scalars(0)
        for h in range(heads):
            for r in range(2):
                send_state(0, r, h)
    for r in range(2):
        for h in range(heads):
            k.exc_t[r * heads + h] = zero_state
    with scope("last_local"):
        start_rims()
        last_local()

    fillers = {0: [("pooling", start_pool)], levels - 1: [("pool_product", pool_product)]}
    fillers.setdefault(max(0, levels - 2), []).append(("backward_enter", backward_enter))
    for level in range(levels):
        final = level + 1 == levels
        if final:
            for name, work in fillers.pop(level, []):
                with scope(name):
                    work()
        with scope(f"scalars{level}"):
            take_scalars(level)
            if not final:
                send_scalars(level + 1)
        for h in range(heads):
            with scope(f"states{level}_{h}"):
                for r in range(2):
                    take_state(level, r, h)
                    if not final:
                        send_state(level + 1, r, h)
            if final:
                with scope(f"finish{h}"):
                    for j, other in enumerate(others):
                        k.mem_out[h, rows_of(other)] = finish(other, h)
                        mem_copies[h][j].start()
                    k.lhs_mem[h, :, own_cols] = finish(group, h)
        if not final:
            for name, work in fillers.pop(level, []):
                with scope(name):
                    work()

    tile = 512
    for h in range(heads):
        with scope(f"wait_mem{h}"):
            for copy in mem_copies[h]:
                copy.wait_recv()
        with scope(f"product{h}"):
            for n in range(model_width // tile):
                cols = slice(n * tile, (n + 1) * tile)
                total = k.acc[:, cols] + jnp.dot(
                    k.lhs_mem[h], k.wmo[h, :, cols], preferred_element_type=F32
                )
                if h + 1 < heads:
                    k.acc[:, cols] = total
                else:
                    k.out[:, cols] = total.astype(BF16)

    for i in range(len(spans)):
        to_far[i].wait_send()
        to_near[i].wait_send()
        onward[i].wait_send()
    for copy in pool_copies + [copy for copies in mem_copies for copy in copies]:
        copy.wait_send()
    for level in range(levels):
        for r in range(2):
            @when(route(level, r)[0])
            def _():
                scalar_copy(level, r).wait_send()
                for h in range(heads):
                    state_copy(level, r, h).wait_send()
    for side in range(2):
        @pl.when(rim_sends[side])
        def _():
            rim(side).wait_send()


def per_device(
    tokens,
    input_norm_gain,
    pooling_input_matrix,
    query_projection_matrix,
    key_projection_matrix,
    value_projection_matrix,
    output_gate_matrix,
    input_gate_matrix,
    forget_gate_matrix,
    forget_gate_bias,
    log_forget_scale,
    extra_log_forget,
    starting_memory,
    starting_normalizer,
    starting_log_scale,
    pooling_group_map,
    pooling_channel_scale,
    memory_head_gain,
    pooling_output_matrix,
    memory_output_matrix,
):
    rows, own_width = tokens.shape
    tp_size = lax.axis_size("tp")
    sp_size = lax.axis_size("sp")
    model_width = own_width * tp_size
    group_dim = pooling_input_matrix.shape[1]
    heads = query_projection_matrix.shape[1] // DH
    mem_width = heads * DH
    pairs = 2 * heads
    levels = max(1, (sp_size - 1).bit_length())
    blocks = tp_size
    size = rows // blocks
    pool_total = pooling_output_matrix.shape[0]
    mem_total = memory_output_matrix.shape[0]
    hbm = pl.BlockSpec(memory_space=pltpu.HBM)
    dma = pltpu.SemaphoreType.DMA
    small = dict(
        gin=input_gate_matrix.transpose(1, 2, 0),
        gfg=forget_gate_matrix.transpose(1, 2, 0),
        gain=input_norm_gain.reshape(1, model_width),
        scale=log_forget_scale,
        extra=extra_log_forget,
        bias=forget_gate_bias,
        start_mem=starting_memory,
        start_norm=starting_normalizer,
        start_log=starting_log_scale,
        map=pooling_group_map,
        pscale=pooling_channel_scale.reshape(1, pool_total),
        hgain=memory_head_gain.reshape(1, mem_total),
    )
    inputs = dict(
        tokens=tokens,
        **{name + "_in": small[name] for name in SMALL},
        wp_hbm=pooling_input_matrix,
        wq_hbm=query_projection_matrix,
        wk_hbm=key_projection_matrix,
        wv_hbm=value_projection_matrix,
        wo_hbm=output_gate_matrix,
        wpo_hbm=pooling_output_matrix,
        wmo_hbm=memory_output_matrix,
    )
    scratch = dict(
        **{name: VMEM(small[name].shape, small[name].dtype) for name in SMALL},
        own=VMEM((rows, own_width), BF16),
        held=VMEM((3, rows, own_width), BF16),
        normed=VMEM((size, model_width), BF16),
        wpg=VMEM((model_width, group_dim + 128), BF16),
        wq=VMEM((model_width, mem_width), BF16),
        wk=VMEM((model_width, mem_width), BF16),
        wv=VMEM((model_width, mem_width), BF16),
        wo=VMEM((model_width, mem_width), BF16),
        wpo=VMEM((pool_total, model_width), BF16),
        wmo=VMEM((heads, tp_size * DH, model_width), BF16),
        lhs_mem=VMEM((heads, size, tp_size * DH), BF16),
        acc=VMEM((size, model_width), F32),
        sums=VMEM((size, 2 * size), BF16),
        ext=VMEM((rows + 2 * RIM, group_dim), F32),
        q=VMEM((rows, mem_width), BF16),
        k=VMEM((rows, mem_width), BF16),
        v=VMEM((rows, mem_width), BF16),
        o=VMEM((rows, mem_width), BF16),
        gates=VMEM((2 * pairs, size), F32),
        lifted=VMEM((pairs, size), F32),
        vt=VMEM((heads, AUG, size), BF16),
        adds=VMEM((heads, blocks, AUG, DH), F32),
        ends=VMEM((blocks, 2 * pairs, 128), F32),
        fcum=VMEM((blocks, pairs, 128), F32),
        peaks=VMEM((blocks, pairs, size), F32),
        locals=VMEM((pairs, blocks, AUG, size), F32),
        gated=VMEM((heads, blocks, DH, size), F32),
        cur_t=VMEM((pairs, AUG, DH), F32),
        cur_s=VMEM((2 * pairs, 128), F32),
        enter_t=VMEM((1, heads, AUG, DH), BF16),
        enter_s=VMEM((1, heads, 128), F32),
        back_t=VMEM((heads, blocks, AUG, DH), BF16),
        back_f=VMEM((heads, AUG, DH), F32),
        back_s=VMEM((blocks, heads, 128), F32),
        inc_s=VMEM((2, 2 * heads, 128), F32),
        exc_t=VMEM((pairs, AUG, DH), F32),
        exc_s=VMEM((2, 2 * heads, 128), F32),
        weigh=VMEM((2, 4 * heads, 128), F32),
        send_t=VMEM((levels, 2, heads, AUG, DH), BF16),
        send_s=VMEM((levels, 2, 2 * heads, 128), F32),
        recv_t=VMEM((levels, 2, heads, AUG, DH), BF16),
        recv_s=VMEM((levels, 2, 2 * heads, 128), F32),
        rim_out=VMEM((2, RIM, group_dim), BF16),
        rims=VMEM((2, RIM, group_dim), BF16),
        pool_out=VMEM((rows, group_dim), BF16),
        mem_out=VMEM((heads, rows, DH), BF16),
        lhs_pool=VMEM((size, pool_total), BF16),
        token_sem=dma((blocks + 1,)),
        load_sem=dma((5,)),
        late_sem=dma((1 + heads * tp_size,)),
        small_sem=dma((len(SMALL),)),
        far_send=dma((blocks + 1,)),
        far_recv=dma((blocks + 1,)),
        near_send=dma((blocks + 1,)),
        near_recv=dma((blocks + 1,)),
        pass_send=dma((blocks + 1,)),
        pass_recv=dma((blocks + 1,)),
        ts=dma((levels, 2, heads)),
        tr=dma((levels, 2, heads)),
        ss=dma((levels, 2)),
        sr=dma((levels, 2)),
        rs=dma((2,)),
        rr=dma((2,)),
        ps=dma((3,)),
        pr=dma((3,)),
        ms=dma((heads, 3)),
        mr=dma((heads, 3)),
    )
    names = tuple(inputs) + ("out",) + tuple(scratch)
    return pl.pallas_call(
        functools.partial(layer_kernel, tp_size, sp_size, heads, names),
        out_shape=VMEM((size, model_width), BF16),
        in_specs=[hbm] * len(inputs),
        out_specs=pl.BlockSpec(memory_space=pltpu.VMEM),
        scratch_shapes=list(scratch.values()),
        compiler_params=pltpu.CompilerParams(
            collective_id=0, has_side_effects=True, vmem_limit_bytes=KERNEL_VMEM
        ),
    )(*(pltpu.with_memory_space_constraint(value, pltpu.HBM) for value in inputs.values()))


def solution(mesh):
    placed = (
        P("sp", "tp"),
        P(),
        P(None, "tp"),
        P(None, "tp"),
        P(None, "tp"),
        P(None, "tp"),
        P(None, "tp"),
        P(),
        P(),
        P(),
        P(None, "sp"),
        P(None, "sp"),
        P(None, "tp", None, None),
        P(None, "tp", None),
        P(None, "tp"),
        P(),
        P(),
        P(),
        P(),
        P(),
    )
    return jax.shard_map(
        per_device, mesh=mesh, in_specs=placed, out_specs=P(("sp", "tp"), None), check_vma=False
    )
```

time: 63.2 us -> 52.8 us (0.84)
  Pallas kernels: 60.7 us -> 51.6 us
  local copies, waits for them, and re-layouts: 2.3 us -> 0.97 us
    pallas_call x1, Pallas kernels: 60.7 us -> 51.6 us  [per_device(): pl.pallas_call(functools.partial(layer_kernel, tp_size, sp_size, heads, n...]
    unnamed x1, local copies, waits for them, and re-layouts: 2.3 us -> 0.97 us
where the time goes in v1:
time: 52.8 us; the launch traced here: 52.6 us
  Pallas kernels  51.6 us (98%)
  local copies, waits for them, and re-layouts  0.97 us (2%)
    pallas_call x1, Pallas kernels, per_device(): pl.pallas_call(functools.partial(layer_kernel, tp_size, sp_size, heads, n...  51.6 us

profile of v1, /device:TPU:1, one launch (start us, length us, event | category | flops | bytes accessed | tf_op | source)
XLA Modules:
  0.0 52.6 jit_solution(18298083794667200202)
XLA Ops:
  0.0 51.6 %shard_map.190 = bf16[256,2048]{1,0:T(8,128)(2,1)S(1)} custom-call(bf16[1024,512]{1,0:T(8,128)(2,1)} %refs_0_.1, bf16[2,8,2048]{2,1,0:T(8,128)(2,1)} %bitcast.5, bf16[2,8,2048]{2,1,0:T(8,128)(2,1)} %bitcast.6, f32[1,2048]{1,0:T(1,128)} %bitcast.7, f32[2,1024]{1,0:T(2,128)} %refs_4_.1, f32[2,1024]{1,0:T(2,128)} %refs_5_.1, f32[2,8]{1,0:T(2,128)} %refs_6_.1, ...), custom_call_target="tpu_custom_call" | custom-call | tf_op jit(solution)/shard_map/pallas_call | solution.py:852
  51.6 1.0 %copy.22 = bf16[256,2048]{1,0:T(8,128)(2,1)} copy(bf16[256,2048]{1,0:T(8,128)(2,1)S(1)} %shard_map.190) | data formatting | bytes 2097152

commit v2 on v1

--- a/solution.py
+++ b/solution.py
@@ -86,9 +86,14 @@
         stride = strides[level]
         if level == 0:
             return True, partner, True
-        if r == 0:
-            return me + stride < sp_size, me + stride, me >= stride
-        return me >= stride, me - stride, me + stride < sp_size
+        step = stride * (1 - 2 * r)
+        target, source = me + step, me - step
+        okay = jnp.logical_and(target >= 0, target < sp_size)
+        has = jnp.logical_and(source >= 0, source < sp_size)
+        return okay, target, has
+
+    late_half = (me >= sp_size // 2).astype(jnp.int32)
+    leading = (late_half, 1 - late_half)
 
     def when(condition):
         if condition is True:
@@ -116,30 +121,32 @@
     spans += [(last * size, half), (last * size + half, half)]
     token_loads = [
         pltpu.make_async_copy(k.tokens.at[pl.ds(a, n)], k.own.at[pl.ds(a, n)], k.token_sem.at[i])
-        for i, (a, n) in enumerate(spans)
+        for i, (a, n) in enumerate(((0, size), (size, rows_total - size)))
     ]
     for load in token_loads:
         load.start()
 
-    def load_group(pairs_of, sems, first=0):
-        copies = [
-            pltpu.make_async_copy(source, target, sems.at[first + i])
-            for i, (source, target) in enumerate(pairs_of)
-        ]
-        for copy in copies:
-            copy.start()
-        return copies
-
-    smalls = load_group(small_refs, k.small_sem)
-    loads = load_group(
-        (
-            (k.wp_hbm, k.wpg.at[:, pl.ds(0, group_dim)]),
-            (k.wk_hbm, k.wk), (k.wv_hbm, k.wv), (k.wq_hbm, k.wq), (k.wo_hbm, k.wo),
-        ),
-        k.load_sem,
+    def load_all(pairs_of, semaphore):
+        for source, target in pairs_of:
+            pltpu.make_async_copy(source, target, semaphore).start()
+
+    def wait_for(ref, semaphore):
+        pltpu.make_async_copy(ref, ref, semaphore).wait()
+
+    smalls = [
+        pltpu.make_async_copy(source, target, k.small_sem.at[i])
+        for i, (source, target) in enumerate(small_refs)
+    ]
+    for load in smalls:
+        load.start()
+    pool_weight = pltpu.make_async_copy(
+        k.wp_hbm, k.wpg.at[:, pl.ds(0, group_dim)], k.load_sem.at[0]
     )
-    for load in smalls[:2]:
-        load.wait()
+    pool_weight.start()
+    wk, wv, wq, wo = (k.weights.at[i] for i in range(4))
+    load_all(
+        ((k.wk_hbm, wk), (k.wv_hbm, wv), (k.wq_hbm, wq), (k.wo_hbm, wo)), k.load_sem.at[1]
+    )
 
     def own_rows(ref, r):
         mine = ref[r, 0:heads, :].astype(F32)
@@ -149,18 +156,6 @@
             )
         return mine
 
-    gate_rows = jnp.concatenate([own_rows(ref, r) for ref in (k.gin, k.gfg) for r in range(2)], axis=0)
-    gate_rows = jnp.concatenate(
-        [gate_rows, jnp.zeros((128 - 2 * pairs, model_width), F32)], axis=0
-    )
-    for n in range(model_width // 128):
-        at = slice(n * 128, (n + 1) * 128)
-        k.wpg[at, group_dim : group_dim + 128] = jnp.transpose(gate_rows[:, at]).astype(BF16)
-    s_at = lax.broadcasted_iota(jnp.int32, (size, size), 0)
-    t_at = lax.broadcasted_iota(jnp.int32, (size, size), 1)
-    k.sums[:, 0:size] = (s_at <= t_at).astype(F32).astype(BF16)
-    k.sums[:, size : 2 * size] = (s_at >= t_at).astype(F32).astype(BF16)
-
     with scope("barrier"):
         pl.semaphore_wait(barrier, peers)
 
@@ -176,26 +171,29 @@
             device_id={"sp": other}, device_id_type=MESH,
         )
 
-    to_far, to_near, onward = [], [], []
+    to_far, onward = [], []
+    to_near = to_tp(k.own, k.held.at[0], k.tp_send, k.near_recv, near)
     for i, (a, n) in enumerate(spans):
         s = pl.ds(a, n)
-        to_far.append(to_tp(k.own.at[s], k.held.at[1, s], k.far_send.at[i], k.far_recv.at[i], far))
-        to_near.append(to_tp(k.own.at[s], k.held.at[0, s], k.near_send.at[i], k.near_recv.at[i], near))
+        to_far.append(to_tp(k.own.at[s], k.held.at[1, s], k.tp_send, k.far_recv.at[i], far))
         onward.append(
-            to_tp(k.held.at[1, s], k.held.at[2, s], k.pass_send.at[i], k.pass_recv.at[i], near)
-        )
-    for i in range(len(spans)):
-        token_loads[i].wait()
-        to_far[i].start()
-    for i in range(len(spans)):
-        to_near[i].start()
+            to_tp(k.held.at[1, s], k.held.at[2, s], k.tp_send, k.pass_recv.at[i], near)
+        )
+    token_loads[0].wait()
+    to_far[0].start()
+    token_loads[1].wait()
+    for copy in to_far[1:]:
+        copy.start()
+    to_near.start()
     mem_rows = [
         (k.wmo_hbm.at[pl.ds((g * heads + h) * DH, DH)], k.wmo.at[h, pl.ds(g * DH, DH)])
         for h in range(heads)
         for g in range(tp_size)
     ]
-    late_loads = load_group([(k.wpo_hbm, k.wpo)] + mem_rows, k.late_sem)
-    for load in smalls[2:]:
+    out_weight = pltpu.make_async_copy(k.wpo_hbm, k.wpo, k.load_sem.at[2])
+    out_weight.start()
+    load_all(mem_rows, k.load_sem.at[3])
+    for load in smalls:
         load.wait()
 
     bias_lane = lax.broadcasted_iota(jnp.int32, k.bias.shape, 1)
@@ -204,6 +202,20 @@
         for h in range(heads)
     ]
     bias = jnp.concatenate([picked[h][r : r + 1] for r in range(2) for h in range(heads)], axis=0)
+
+    s_at = lax.broadcasted_iota(jnp.int32, (size, size), 0)
+    t_at = lax.broadcasted_iota(jnp.int32, (size, size), 1)
+
+    def gate_weights():
+        gate_rows = jnp.concatenate([own_rows(ref, r) for ref in (k.gin, k.gfg) for r in range(2)], axis=0)
+        gate_rows = jnp.concatenate(
+            [gate_rows, jnp.zeros((128 - 2 * pairs, model_width), F32)], axis=0
+        )
+        for n in range(model_width // 128):
+            at = slice(n * 128, (n + 1) * 128)
+            k.wpg[at, group_dim : group_dim + 128] = jnp.transpose(gate_rows[:, at]).astype(BF16)
+        k.sums[:, 0:size] = (s_at <= t_at).astype(F32).astype(BF16)
+        k.sums[:, size : 2 * size] = (s_at >= t_at).astype(F32).astype(BF16)
 
     def both_rows(ref, span):
         return jnp.concatenate(
@@ -371,34 +383,55 @@
             k.gated[h, b] = wide(column, size) / (1.0 + jnp.exp(-opened))
 
     with scope("prepare"):
+        gate_weights()
         prepare()
+    def rim(side):
+        other = me + 1 if side == 0 else me - 1
+        return to_sp(k.rim_out.at[side], k.rims.at[side], k.rs.at[side], k.rr.at[side], other)
+
+    def start_rims():
+        k.rim_out[1] = k.ext[RIM : 2 * RIM, :].astype(BF16)
+        k.rim_out[0] = k.ext[rows_total : RIM + rows_total, :].astype(BF16)
+        for side in range(2):
+            @pl.when(rim_sends[side])
+            def _():
+                rim(side).start()
+
+    def pass_on(i):
+        to_far[i].wait_recv()
+        onward[i].start()
+
     for b in range(blocks):
         pieces = [i for i, (a, n) in enumerate(spans) if b * size <= a < (b + 1) * size]
         with scope(f"far{b}"):
-            for i in pieces:
-                to_far[i].wait_recv()
-                onward[i].start()
+            for i in pieces[1 if b == last and b > 0 else 0 :]:
+                pass_on(i)
         for i in pieces:
             a, n = spans[i]
             at = a - b * size
+            if i == 0:
+                to_near.wait_recv()
             with scope(f"wait{i}"):
-                to_near[i].wait_recv()
                 onward[i].wait_recv()
             if i == 0:
-                for load in loads:
-                    load.wait()
+                pool_weight.wait()
+                wait_for(k.weights, k.load_sem.at[1])
             with scope(f"project{i}"):
                 normalize(a, n, at)
                 project_gates(a, n, at)
-                project(a, n, at, ((k.wk, k.k), (k.wv, k.v)))
+                project(a, n, at, ((wk, k.k), (wv, k.v)))
+        if b == last - 1:
+            with scope("far_half"):
+                pass_on(last)
         if b < last:
             with scope(f"local{b}"):
-                project(b * size, size, 0, ((k.wq, k.q), (k.wo, k.o)))
+                project(b * size, size, 0, ((wq, k.q), (wo, k.o)))
                 summary(b)
                 local_block(b)
                 out_gates(b)
         else:
             with scope(f"summary{b}"):
+                start_rims()
                 summary(b)
 
     for r in range(2):
@@ -415,7 +448,7 @@
 
     def state_copy(level, r, h):
         return to_sp(
-            k.send_t.at[level, r, h], k.recv_t.at[level, r, h], k.ts.at[level, r, h],
+            k.send_t.at[level, r, h], k.recv_t.at[level, r, h], k.ts.at[level, r],
             k.tr.at[level, r, h], route(level, r)[1],
         )
 
@@ -492,18 +525,6 @@
                 mine = mine + k.weigh[r, 3 * heads + h : 3 * heads + h + 1, :] * k.exc_t[p]
             k.exc_t[p] = mine
 
-    def rim(side):
-        other = me + 1 if side == 0 else me - 1
-        return to_sp(k.rim_out.at[side], k.rims.at[side], k.rs.at[side], k.rr.at[side], other)
-
-    def start_rims():
-        k.rim_out[1] = k.ext[RIM : 2 * RIM, :].astype(BF16)
-        k.rim_out[0] = k.ext[rows_total : RIM + rows_total, :].astype(BF16)
-        for side in range(2):
-            @pl.when(rim_sends[side])
-            def _():
-                rim(side).start()
-
     def pooling():
         for side in range(2):
             at = 0 if side == 0 else RIM + rows_total
@@ -549,14 +570,14 @@
     own_cols = pl.ds(pl.multiple_of(group * DH, DH), DH)
 
     pool_copies = [
-        to_tp(k.pool_out.at[rows_of(other)], k.lhs_pool.at[:, pool_cols], k.ps.at[j], k.pr.at[j], other)
+        to_tp(k.pool_out.at[rows_of(other)], k.lhs_pool.at[:, pool_cols], k.pool_send, k.pr, other)
         for j, other in enumerate(others)
     ]
     mem_copies = [
         [
             to_tp(
                 k.mem_out.at[h, rows_of(other)], k.lhs_mem.at[h, :, own_cols],
-                k.ms.at[h, j], k.mr.at[h, j], other,
+                k.mem_send, k.mr.at[h], other,
             )
             for j, other in enumerate(others)
         ]
@@ -570,14 +591,12 @@
 
     def pool_product():
         k.lhs_pool[:, pool_cols] = k.pool_out[rows_of(group), :]
-        for copy in pool_copies:
-            copy.wait_recv()
-        for load in late_loads:
-            load.wait()
+        wait_for(k.pool_out.at[pl.ds(0, len(others) * size)], k.pr)
+        out_weight.wait()
         k.acc[...] = jnp.dot(k.lhs_pool[...], k.wpo[...], preferred_element_type=F32)
 
     def last_local():
-        project(last * size, size, 0, ((k.wq, k.q), (k.wo, k.o)))
+        project(last * size, size, 0, ((wq, k.q), (wo, k.o)))
         local_block(last)
         out_gates(last)
 
@@ -643,49 +662,62 @@
     with scope("send0"):
         send_scalars(0)
         for h in range(heads):
-            for r in range(2):
+            for r in leading:
                 send_state(0, r, h)
     for r in range(2):
         for h in range(heads):
             k.exc_t[r * heads + h] = zero_state
     with scope("last_local"):
-        start_rims()
         last_local()
 
-    fillers = {0: [("pooling", start_pool)], levels - 1: [("pool_product", pool_product)]}
-    fillers.setdefault(max(0, levels - 2), []).append(("backward_enter", backward_enter))
+    def settle(level):
+        for r in range(2):
+            @when(route(level, r)[0])
+            def _():
+                scalar_copy(level, r).wait_send()
+                wait_for(k.send_t.at[level, r], k.ts.at[level, r])
+
     for level in range(levels):
         final = level + 1 == levels
         if final:
-            for name, work in fillers.pop(level, []):
-                with scope(name):
-                    work()
+            if level == 0:
+                start_pool()
+            with scope("backward_enter"):
+                backward_enter()
         with scope(f"scalars{level}"):
             take_scalars(level)
             if not final:
                 send_scalars(level + 1)
         for h in range(heads):
             with scope(f"states{level}_{h}"):
-                for r in range(2):
+                for r in leading:
                     take_state(level, r, h)
                     if not final:
                         send_state(level + 1, r, h)
             if final:
                 with scope(f"finish{h}"):
-                    for j, other in enumerate(others):
-                        k.mem_out[h, rows_of(other)] = finish(other, h)
+                    for j in range(2):
+                        k.mem_out[h, rows_of(others[j])] = finish(others[j], h)
                         mem_copies[h][j].start()
-                    k.lhs_mem[h, :, own_cols] = finish(group, h)
-        if not final:
-            for name, work in fillers.pop(level, []):
-                with scope(name):
-                    work()
+            elif level == 0 and h == 0:
+                with scope("pooling"):
+                    start_pool()
+    with scope("finish_near"):
+        for h in range(heads):
+            k.mem_out[h, rows_of(near)] = finish(near, h)
+            mem_copies[h][2].start()
+    with scope("finish_own"):
+        for h in range(heads):
+            k.lhs_mem[h, :, own_cols] = finish(group, h)
+    with scope("pool_product"):
+        pool_product()
 
     tile = 512
     for h in range(heads):
         with scope(f"wait_mem{h}"):
-            for copy in mem_copies[h]:
-                copy.wait_recv()
+            wait_for(k.mem_out.at[h, pl.ds(0, len(others) * size)], k.mr.at[h])
+            if h == 0:
+                wait_for(k.wmo, k.load_sem.at[3])
         with scope(f"product{h}"):
             for n in range(model_width // tile):
                 cols = slice(n * tile, (n + 1) * tile)
@@ -697,23 +729,16 @@
                 else:
                     k.out[:, cols] = total.astype(BF16)
 
-    for i in range(len(spans)):
-        to_far[i].wait_send()
-        to_near[i].wait_send()
-        onward[i].wait_send()
-    for copy in pool_copies + [copy for copies in mem_copies for copy in copies]:
-        copy.wait_send()
-    for level in range(levels):
-        for r in range(2):
-            @when(route(level, r)[0])
+    with scope("leave"):
+        wait_for(k.held, k.tp_send)
+        wait_for(k.pool_out.at[pl.ds(0, len(others) * size)], k.pool_send)
+        wait_for(k.mem_out.at[:, pl.ds(0, len(others) * size)], k.mem_send)
+        for level in range(levels):
+            settle(level)
+        for side in range(2):
+            @pl.when(rim_sends[side])
             def _():
-                scalar_copy(level, r).wait_send()
-                for h in range(heads):
-                    state_copy(level, r, h).wait_send()
-    for side in range(2):
-        @pl.when(rim_sends[side])
-        def _():
-            rim(side).wait_send()
+                rim(side).wait_send()
 
 
 def per_device(
@@ -784,10 +809,7 @@
         held=VMEM((3, rows, own_width), BF16),
         normed=VMEM((size, model_width), BF16),
         wpg=VMEM((model_width, group_dim + 128), BF16),
-        wq=VMEM((model_width, mem_width), BF16),
-        wk=VMEM((model_width, mem_width), BF16),
-        wv=VMEM((model_width, mem_width), BF16),
-        wo=VMEM((model_width, mem_width), BF16),
+        weights=VMEM((4, model_width, mem_width), BF16),
         wpo=VMEM((pool_total, model_width), BF16),
         wmo=VMEM((heads, tp_size * DH, model_width), BF16),
         lhs_mem=VMEM((heads, size, tp_size * DH), BF16),
@@ -827,26 +849,23 @@
         pool_out=VMEM((rows, group_dim), BF16),
         mem_out=VMEM((heads, rows, DH), BF16),
         lhs_pool=VMEM((size, pool_total), BF16),
-        token_sem=dma((blocks + 1,)),
-        load_sem=dma((5,)),
-        late_sem=dma((1 + heads * tp_size,)),
+        token_sem=dma((2,)),
         small_sem=dma((len(SMALL),)),
-        far_send=dma((blocks + 1,)),
+        load_sem=dma((4,)),
+        tp_send=dma,
+        pool_send=dma,
+        mem_send=dma,
+        near_recv=dma,
         far_recv=dma((blocks + 1,)),
-        near_send=dma((blocks + 1,)),
-        near_recv=dma((blocks + 1,)),
-        pass_send=dma((blocks + 1,)),
         pass_recv=dma((blocks + 1,)),
-        ts=dma((levels, 2, heads)),
+        ts=dma((levels, 2)),
         tr=dma((levels, 2, heads)),
         ss=dma((levels, 2)),
         sr=dma((levels, 2)),
         rs=dma((2,)),
         rr=dma((2,)),
-        ps=dma((3,)),
-        pr=dma((3,)),
-        ms=dma((heads, 3)),
-        mr=dma((heads, 3)),
+        pr=dma,
+        mr=dma((heads,)),
     )
     names = tuple(inputs) + ("out",) + tuple(scratch)
     return pl.pallas_call(

time: 52.8 us -> 51.4 us (0.973)
  Pallas kernels: 51.6 us -> 50.3 us
    pallas_call x1, Pallas kernels: 51.6 us -> 50.3 us  [per_device(): pl.pallas_call(functools.partial(layer_kernel, tp_size, sp_size, heads, n...]
where the time goes in v2:
time: 51.4 us; the launch traced here: 51.2 us
  Pallas kernels  50.3 us (98%)
  local copies, waits for them, and re-layouts  0.97 us (2%)
    pallas_call x1, Pallas kernels, per_device(): pl.pallas_call(functools.partial(layer_kernel, tp_size, sp_size, heads, n...  50.3 us

profile of v2, /device:TPU:1, one launch (start us, length us, event | category | flops | bytes accessed | tf_op | source)
XLA Modules:
  0.0 51.2 jit_solution(8240070839479128160)
XLA Ops:
  0.0 50.3 %shard_map.190 = bf16[256,2048]{1,0:T(8,128)(2,1)S(1)} custom-call(bf16[1024,512]{1,0:T(8,128)(2,1)} %refs_0_.1, bf16[2,8,2048]{2,1,0:T(8,128)(2,1)} %bitcast.5, bf16[2,8,2048]{2,1,0:T(8,128)(2,1)} %bitcast.6, f32[1,2048]{1,0:T(1,128)} %bitcast.7, f32[2,1024]{1,0:T(2,128)} %refs_4_.1, f32[2,1024]{1,0:T(2,128)} %refs_5_.1, f32[2,8]{1,0:T(2,128)} %refs_6_.1, ...), custom_call_target="tpu_custom_call" | custom-call | tf_op jit(solution)/shard_map/pallas_call | solution.py:871
  50.3 1.0 %copy.22 = bf16[256,2048]{1,0:T(8,128)(2,1)} copy(bf16[256,2048]{1,0:T(8,128)(2,1)S(1)} %shard_map.190) | data formatting | bytes 2097152

commit v3 on v2

--- a/solution.py
+++ b/solution.py
@@ -133,6 +133,43 @@
     def wait_for(ref, semaphore):
         pltpu.make_async_copy(ref, ref, semaphore).wait()
 
+    def own_rows(ref, r):
+        mine = ref[r, 0:heads, :].astype(F32)
+        for other in range(1, tp_size):
+            mine = jnp.where(
+                group == other, ref[r, other * heads : (other + 1) * heads, :].astype(F32), mine
+            )
+        return mine
+
+    with scope("barrier"):
+        pl.semaphore_wait(barrier, peers)
+
+    def to_tp(source, target, send, recv, other):
+        return pltpu.make_async_remote_copy(
+            src_ref=source, dst_ref=target, send_sem=send, recv_sem=recv,
+            device_id={"tp": other}, device_id_type=MESH,
+        )
+
+    def to_sp(source, target, send, recv, other):
+        return pltpu.make_async_remote_copy(
+            src_ref=source, dst_ref=target, send_sem=send, recv_sem=recv,
+            device_id={"sp": other}, device_id_type=MESH,
+        )
+
+    to_far, onward = [], []
+    to_near = to_tp(k.own, k.held.at[0], k.tp_send, k.near_recv, near)
+    for i, (a, n) in enumerate(spans):
+        s = pl.ds(a, n)
+        to_far.append(to_tp(k.own.at[s], k.held.at[1, s], k.tp_send, k.far_recv.at[i], far))
+        onward.append(
+            to_tp(k.held.at[1, s], k.held.at[2, s], k.tp_send, k.pass_recv.at[i], near)
+        )
+    token_loads[0].wait()
+    to_far[0].start()
+    token_loads[1].wait()
+    for copy in to_far[1:]:
+        copy.start()
+    to_near.start()
     smalls = [
         pltpu.make_async_copy(source, target, k.small_sem.at[i])
         for i, (source, target) in enumerate(small_refs)
@@ -148,43 +185,6 @@
         ((k.wk_hbm, wk), (k.wv_hbm, wv), (k.wq_hbm, wq), (k.wo_hbm, wo)), k.load_sem.at[1]
     )
 
-    def own_rows(ref, r):
-        mine = ref[r, 0:heads, :].astype(F32)
-        for other in range(1, tp_size):
-            mine = jnp.where(
-                group == other, ref[r, other * heads : (other + 1) * heads, :].astype(F32), mine
-            )
-        return mine
-
-    with scope("barrier"):
-        pl.semaphore_wait(barrier, peers)
-
-    def to_tp(source, target, send, recv, other):
-        return pltpu.make_async_remote_copy(
-            src_ref=source, dst_ref=target, send_sem=send, recv_sem=recv,
-            device_id={"tp": other}, device_id_type=MESH,
-        )
-
-    def to_sp(source, target, send, recv, other):
-        return pltpu.make_async_remote_copy(
-            src_ref=source, dst_ref=target, send_sem=send, recv_sem=recv,
-            device_id={"sp": other}, device_id_type=MESH,
-        )
-
-    to_far, onward = [], []
-    to_near = to_tp(k.own, k.held.at[0], k.tp_send, k.near_recv, near)
-    for i, (a, n) in enumerate(spans):
-        s = pl.ds(a, n)
-        to_far.append(to_tp(k.own.at[s], k.held.at[1, s], k.tp_send, k.far_recv.at[i], far))
-        onward.append(
-            to_tp(k.held.at[1, s], k.held.at[2, s], k.tp_send, k.pass_recv.at[i], near)
-        )
-    token_loads[0].wait()
-    to_far[0].start()
-    token_loads[1].wait()
-    for copy in to_far[1:]:
-        copy.start()
-    to_near.start()
     mem_rows = [
         (k.wmo_hbm.at[pl.ds((g * heads + h) * DH, DH)], k.wmo.at[h, pl.ds(g * DH, DH)])
         for h in range(heads)
@@ -222,15 +222,24 @@
             [jnp.broadcast_to(ref[r : r + 1, span], (heads, size)) for r in range(2)], axis=0
         )
 
-    def normalize(a, n, at):
+    def add_sums(sums, view):
+        part = view.astype(F32)
+        return (
+            sums[0] + jnp.sum(part, axis=1, keepdims=True),
+            sums[1] + jnp.sum(part * part, axis=1, keepdims=True),
+        )
+
+    def early_sums(a, n):
+        rows = slice(a, a + n)
+        sums = (jnp.zeros((n, 1), F32), jnp.zeros((n, 1), F32))
+        for view in (k.own[rows, :], k.held[0, rows, :], k.held[1, rows, :]):
+            sums = add_sums(sums, view)
+        return sums
+
+    def normalize(a, n, at, sums):
         rows = slice(a, a + n)
         views = [k.own[rows, :]] + [k.held[slot, rows, :] for slot in range(3)]
-        total = jnp.zeros((n, 1), F32)
-        square = jnp.zeros((n, 1), F32)
-        for view in views:
-            part = view.astype(F32)
-            total = total + jnp.sum(part, axis=1, keepdims=True)
-            square = square + jnp.sum(part * part, axis=1, keepdims=True)
+        total, square = add_sums(sums, views[3])
         mean = total / model_width
         inverse = lax.rsqrt(square / model_width - mean * mean + LN_EPS)
         for view, owner in zip(views, (group, near, far, diagonal)):
@@ -412,12 +421,13 @@
             if i == 0:
                 to_near.wait_recv()
             with scope(f"wait{i}"):
+                sums = early_sums(a, n)
                 onward[i].wait_recv()
             if i == 0:
                 pool_weight.wait()
                 wait_for(k.weights, k.load_sem.at[1])
             with scope(f"project{i}"):
-                normalize(a, n, at)
+                normalize(a, n, at, sums)
                 project_gates(a, n, at)
                 project(a, n, at, ((wk, k.k), (wv, k.v)))
         if b == last - 1:
@@ -577,7 +587,7 @@
         [
             to_tp(
                 k.mem_out.at[h, rows_of(other)], k.lhs_mem.at[h, :, own_cols],
-                k.mem_send, k.mr.at[h], other,
+                k.mem_send, k.mr.at[h] if j < 2 else k.mn.at[h], other,
             )
             for j, other in enumerate(others)
         ]
@@ -589,11 +599,26 @@
         for copy in pool_copies:
             copy.start()
 
-    def pool_product():
+    home = pl.ds(pl.multiple_of(lax.div(group, 2) * 2 * DH, 2 * DH), 2 * DH)
+    away = pl.ds(pl.multiple_of(lax.div(far, 2) * 2 * DH, 2 * DH), 2 * DH)
+    tile = 512
+
+    def mem_product(h, span, cols):
+        return jnp.dot(k.lhs_mem[h, :, span], k.wmo[h, span, cols], preferred_element_type=F32)
+
+    def home_product():
         k.lhs_pool[:, pool_cols] = k.pool_out[rows_of(group), :]
         wait_for(k.pool_out.at[pl.ds(0, len(others) * size)], k.pr)
         out_weight.wait()
-        k.acc[...] = jnp.dot(k.lhs_pool[...], k.wpo[...], preferred_element_type=F32)
+        wait_for(k.wmo, k.load_sem.at[3])
+        for h in range(heads):
+            wait_for(k.mem_out.at[h, pl.ds(0, size)], k.mn.at[h])
+        for n in range(model_width // tile):
+            cols = slice(n * tile, (n + 1) * tile)
+            total = jnp.dot(k.lhs_pool[...], k.wpo[:, cols], preferred_element_type=F32)
+            for h in range(heads):
+                total = total + mem_product(h, home, cols)
+            k.acc[:, cols] = total
 
     def last_local():
         project(last * size, size, 0, ((wq, k.q), (wo, k.o)))
@@ -664,6 +689,7 @@
         for h in range(heads):
             for r in leading:
                 send_state(0, r, h)
+        wait_for(k.held, k.tp_send)
     for r in range(2):
         for h in range(heads):
             k.exc_t[r * heads + h] = zero_state
@@ -699,41 +725,34 @@
                     for j in range(2):
                         k.mem_out[h, rows_of(others[j])] = finish(others[j], h)
                         mem_copies[h][j].start()
+                if h == 0:
+                    settle(0)
+                with scope(f"finish_near{h}"):
+                    k.mem_out[h, rows_of(near)] = finish(near, h)
+                    mem_copies[h][2].start()
+                with scope(f"finish_own{h}"):
+                    k.lhs_mem[h, :, own_cols] = finish(group, h)
             elif level == 0 and h == 0:
                 with scope("pooling"):
                     start_pool()
-    with scope("finish_near"):
-        for h in range(heads):
-            k.mem_out[h, rows_of(near)] = finish(near, h)
-            mem_copies[h][2].start()
-    with scope("finish_own"):
-        for h in range(heads):
-            k.lhs_mem[h, :, own_cols] = finish(group, h)
-    with scope("pool_product"):
-        pool_product()
-
-    tile = 512
+    with scope("home_product"):
+        home_product()
     for h in range(heads):
         with scope(f"wait_mem{h}"):
-            wait_for(k.mem_out.at[h, pl.ds(0, len(others) * size)], k.mr.at[h])
-            if h == 0:
-                wait_for(k.wmo, k.load_sem.at[3])
+            wait_for(k.mem_out.at[h, pl.ds(0, 2 * size)], k.mr.at[h])
         with scope(f"product{h}"):
             for n in range(model_width // tile):
                 cols = slice(n * tile, (n + 1) * tile)
-                total = k.acc[:, cols] + jnp.dot(
-                    k.lhs_mem[h], k.wmo[h, :, cols], preferred_element_type=F32
-                )
+                total = k.acc[:, cols] + mem_product(h, away, cols)
                 if h + 1 < heads:
                     k.acc[:, cols] = total
                 else:
                     k.out[:, cols] = total.astype(BF16)
 
     with scope("leave"):
-        wait_for(k.held, k.tp_send)
         wait_for(k.pool_out.at[pl.ds(0, len(others) * size)], k.pool_send)
         wait_for(k.mem_out.at[:, pl.ds(0, len(others) * size)], k.mem_send)
-        for level in range(levels):
+        for level in range(1, levels):
             settle(level)
         for side in range(2):
             @pl.when(rim_sends[side])
@@ -866,6 +885,7 @@
         rr=dma((2,)),
         pr=dma,
         mr=dma((heads,)),
+        mn=dma((heads,)),
     )
     names = tuple(inputs) + ("out",) + tuple(scratch)
     return pl.pallas_call(

time: 51.4 us -> 50.6 us (0.984)
  Pallas kernels: 50.3 us -> 49.4 us
    pallas_call x1, Pallas kernels: 50.3 us -> 49.4 us  [per_device(): pl.pallas_call(functools.partial(layer_kernel, tp_size, sp_size, heads, n...]
where the time goes in v3:
time: 50.6 us; the launch traced here: 50.4 us
  Pallas kernels  49.4 us (98%)
  local copies, waits for them, and re-layouts  0.97 us (2%)
    pallas_call x1, Pallas kernels, per_device(): pl.pallas_call(functools.partial(layer_kernel, tp_size, sp_size, heads, n...  49.4 us

profile of v3, /device:TPU:1, one launch (start us, length us, event | category | flops | bytes accessed | tf_op | source)
XLA Modules:
  0.0 50.4 jit_solution(14731833486869527817)
XLA Ops:
  0.0 49.4 %shard_map.190 = bf16[256,2048]{1,0:T(8,128)(2,1)S(1)} custom-call(bf16[1024,512]{1,0:T(8,128)(2,1)} %refs_0_.1, bf16[2,8,2048]{2,1,0:T(8,128)(2,1)} %bitcast.5, bf16[2,8,2048]{2,1,0:T(8,128)(2,1)} %bitcast.6, f32[1,2048]{1,0:T(1,128)} %bitcast.7, f32[2,1024]{1,0:T(2,128)} %refs_4_.1, f32[2,1024]{1,0:T(2,128)} %refs_5_.1, f32[2,8]{1,0:T(2,128)} %refs_6_.1, ...), custom_call_target="tpu_custom_call" | custom-call | tf_op jit(solution)/shard_map/pallas_call | solution.py:891
  49.4 1.0 %copy.22 = bf16[256,2048]{1,0:T(8,128)(2,1)} copy(bf16[256,2048]{1,0:T(8,128)(2,1)S(1)} %shard_map.190) | data formatting | bytes 2097152

commit v4 on v3

--- a/solution.py
+++ b/solution.py
@@ -696,8 +696,8 @@
     with scope("last_local"):
         last_local()
 
-    def settle(level):
-        for r in range(2):
+    def settle(level, directions=(0, 1)):
+        for r in directions:
             @when(route(level, r)[0])
             def _():
                 scalar_copy(level, r).wait_send()
@@ -725,8 +725,10 @@
                     for j in range(2):
                         k.mem_out[h, rows_of(others[j])] = finish(others[j], h)
                         mem_copies[h][j].start()
-                if h == 0:
-                    settle(0)
+                        if h == 0:
+                            settle(0, (j,))
+                        elif h == 1 and j == 0:
+                            wait_for(k.pool_out.at[pl.ds(0, len(others) * size)], k.pool_send)
                 with scope(f"finish_near{h}"):
                     k.mem_out[h, rows_of(near)] = finish(near, h)
                     mem_copies[h][2].start()
@@ -750,7 +752,8 @@
                     k.out[:, cols] = total.astype(BF16)
 
     with scope("leave"):
-        wait_for(k.pool_out.at[pl.ds(0, len(others) * size)], k.pool_send)
+        if heads < 2:
+            wait_for(k.pool_out.at[pl.ds(0, len(others) * size)], k.pool_send)
         wait_for(k.mem_out.at[:, pl.ds(0, len(others) * size)], k.mem_send)
         for level in range(1, levels):
             settle(level)

time: 50.6 us -> 50.6 us (level)
  no operation moved by 1% of the time
where the time goes in v4:
time: 50.6 us; the launch traced here: 50.4 us
  Pallas kernels  49.4 us (98%)
  local copies, waits for them, and re-layouts  0.97 us (2%)
    pallas_call x1, Pallas kernels, per_device(): pl.pallas_call(functools.partial(layer_kernel, tp_size, sp_size, heads, n...  49.4 us

profile of v4, /device:TPU:1, one launch (start us, length us, event | category | flops | bytes accessed | tf_op | source)
XLA Modules:
  0.0 50.4 jit_solution(6202614746640117772)
XLA Ops:
  0.0 49.4 %shard_map.190 = bf16[256,2048]{1,0:T(8,128)(2,1)S(1)} custom-call(bf16[1024,512]{1,0:T(8,128)(2,1)} %refs_0_.1, bf16[2,8,2048]{2,1,0:T(8,128)(2,1)} %bitcast.5, bf16[2,8,2048]{2,1,0:T(8,128)(2,1)} %bitcast.6, f32[1,2048]{1,0:T(1,128)} %bitcast.7, f32[2,1024]{1,0:T(2,128)} %refs_4_.1, f32[2,1024]{1,0:T(2,128)} %refs_5_.1, f32[2,8]{1,0:T(2,128)} %refs_6_.1, ...), custom_call_target="tpu_custom_call" | custom-call | tf_op jit(solution)/shard_map/pallas_call | solution.py:894
  49.4 1.0 %copy.22 = bf16[256,2048]{1,0:T(8,128)(2,1)} copy(bf16[256,2048]{1,0:T(8,128)(2,1)S(1)} %shard_map.190) | data formatting | bytes 2097152
